TPU v7x, 256 devices: a whole 4x4x8 slice. The times are simulated.
256 devices in a mesh: sp: 32 (over z, x), tp: 8 (over y, core).
Axes of the slice: x: 4, y: 4, z: 8, core: 2. Of those that a mesh axis runs over, the one named last changes fastest.
Arguments:
- tokens: bfloat16 [12288, 2048], P(('sp', 'tp')), may hold values from -6 to 6
- norm_gain: bfloat16 [2048], replicated, may hold values from 0.099609375 to 1.8984375
- query_down_weight: bfloat16 [2048, 512], replicated, may hold values from -0.125 to 0.125
- query_latent_norm_gain: bfloat16 [512], replicated, may hold values from 0.099609375 to 1.8984375
- key_value_down_weight: bfloat16 [2048, 256], replicated, may hold values from -0.125 to 0.125
- key_value_latent_gain: bfloat16 [256], replicated, may hold values from 0.099609375 to 1.8984375
- w_rope_key: bfloat16 [2048, 32], replicated, may hold values from -0.125 to 0.125
- w_pool_in: bfloat16 [2048, 512], replicated, may hold values from -0.125 to 0.125
- query_up_weight: bfloat16 [512, 2304], P(None, 'tp'), may hold values from -0.25 to 0.25
- key_value_up_weight: bfloat16 [256, 3072], P(None, 'tp'), may hold values from -0.375 to 0.375
- query_gain: bfloat16 [96], replicated, may hold values from 1 to 16
- key_gain: bfloat16 [96], replicated, may hold values from 1 to 16
- w_pool_mix: bfloat16 [8, 64, 64], P('tp'), may hold values from -0.75 to 0.75
- pool_scale: bfloat16 [512], P('tp'), may hold values from 1 to 10
- w_out_attn: bfloat16 [1536, 2048], P('tp'), may hold values from -0.3125 to 0.3125
- w_out_pool: bfloat16 [512, 2048], P('tp'), may hold values from -0.25 to 0.25
Outputs:
- mixed: bfloat16 [12288, 2048], P(('sp', 'tp'))
- row_logsum: float32 [24, 12288], P('tp', 'sp')
All inputs are finite; a program needn't handle non-finite values.
Results may differ from a plain program's by a relative error of at most 0.035.
Values may be sent and summed in bfloat16 or wider, within the bound.
A program may use at most 128 MiB of HBM per device.

v0:
```python
import jax
import jax.numpy as jnp
from jax import lax
from jax.sharding import PartitionSpec as P

PLAIN_HEAD_SIZE = 64
ROTARY_SIZE = 32
VALUE_HEAD_SIZE = 64
QUERY_RANK = 512
KEY_VALUE_RANK = 256
GDIM = 64


epsilon = 1e-06
rope_base = 10000.0
rim_width = 8


def from_everyone(x, axis):
    count = lax.axis_size(axis)
    return lax.all_to_all(jnp.broadcast_to(x[None], (count, *x.shape)), axis, 0, 0, tiled=True)


def in_order(pieces, dim):
    shape = list(pieces.shape[1:])
    shape[dim] *= pieces.shape[0]
    return jnp.moveaxis(pieces, 0, dim).reshape(shape)


def gathered_copies(x, axis, dim):
    pieces = from_everyone(x, axis)
    return in_order(pieces, dim)


def with_halo(block, sides, width):
    for axis, dim in sides:
        count = lax.axis_size(axis)
        forward = [(i, i + 1) for i in range(count - 1)]
        backward = [(target, source) for source, target in forward]
        low = lax.ppermute(
            lax.slice_in_dim(block, block.shape[dim] - width, None, axis=dim), axis, forward
        )
        high = lax.ppermute(lax.slice_in_dim(block, 0, width, axis=dim), axis, backward)
        block = jnp.concatenate([low, block, high], axis=dim)
    return block


def cut_along(x, dim, count):
    shape = x.shape
    pieces = x.reshape(*shape[:dim], count, shape[dim] // count, *shape[dim + 1 :])
    return jnp.moveaxis(pieces, dim, 0)


def sent_and_summed(x, axis, dim):
    count = lax.axis_size(axis)
    pieces = lax.all_to_all(cut_along(x, dim, count), axis, 0, 0, tiled=True)
    return jnp.sum(pieces.astype(jnp.float32), axis=0)


def norm_rows(values, gain):
    mean_square = jnp.mean(values * values, axis=-1, keepdims=True)
    return values * lax.rsqrt(mean_square + epsilon) * gain.astype(jnp.float32)


def rotate_tail(values, positions):
    half = ROTARY_SIZE // 2
    freqs = rope_base ** (-jnp.arange(half, dtype=jnp.float32) / half)
    angles = positions[:, None] * freqs[None, :]
    cosine = jnp.cos(angles)[:, None, :]
    sine = jnp.sin(angles)[:, None, :]
    first = values[..., PLAIN_HEAD_SIZE : PLAIN_HEAD_SIZE + half]
    second = values[..., PLAIN_HEAD_SIZE + half :]
    return jnp.concatenate(
        [
            values[..., :PLAIN_HEAD_SIZE],
            first * cosine - second * sine,
            first * sine + second * cosine,
        ],
        axis=-1,
    )


def shards(
    tokens,
    norm_gain,
    query_down_weight,
    query_latent_norm_gain,
    key_value_down_weight,
    key_value_latent_gain,
    w_rope_key,
    w_pool_in,
    query_up_weight,
    key_value_up_weight,
    query_gain,
    key_gain,
    w_pool_mix,
    pool_scale,
    w_out_attn,
    w_out_pool,
):
    sp_count = lax.axis_size("sp")
    local_heads = query_up_weight.shape[1] // (PLAIN_HEAD_SIZE + ROTARY_SIZE)
    groups_here = w_pool_mix.shape[0]
    pool_cols = groups_here * GDIM
    latent_columns = QUERY_RANK + KEY_VALUE_RANK + ROTARY_SIZE
    pool_weight = lax.dynamic_slice_in_dim(
        w_pool_in, lax.axis_index("tp") * pool_cols, pool_cols, 1
    )
    normed = norm_rows(gathered_copies(tokens, "tp", 0).astype(jnp.float32), norm_gain).astype(
        jnp.bfloat16
    )
    pool_part = jnp.dot(normed, pool_weight, preferred_element_type=jnp.float32).astype(
        jnp.bfloat16
    )
    query_part = norm_rows(
        jnp.dot(normed, query_down_weight, preferred_element_type=jnp.float32),
        query_latent_norm_gain,
    )
    kv_part = norm_rows(
        jnp.dot(normed, key_value_down_weight, preferred_element_type=jnp.float32),
        key_value_latent_gain,
    )
    rope_part = jnp.dot(normed, w_rope_key, preferred_element_type=jnp.float32)
    projected = jnp.concatenate(
        [
            jnp.concatenate(
                [
                    query_part.astype(jnp.bfloat16),
                    kv_part.astype(jnp.bfloat16),
                    rope_part.astype(jnp.bfloat16),
                ],
                axis=1,
            ),
            pool_part,
        ],
        axis=1,
    )
    latent_vectors = projected[:, :latent_columns]
    pool_input = projected[:, latent_columns:]
    rows = latent_vectors.shape[0]
    offset = lax.axis_index("sp") * rows
    places = offset + jnp.arange(rows, dtype=jnp.int32)
    positions = places.astype(jnp.float32)
    query_vectors = jnp.dot(
        latent_vectors[:, :QUERY_RANK], query_up_weight, preferred_element_type=jnp.float32
    ).reshape(rows, local_heads, PLAIN_HEAD_SIZE + ROTARY_SIZE)
    query_vectors = rotate_tail(norm_rows(query_vectors, query_gain), positions).astype(
        jnp.bfloat16
    )
    key_value_rows = latent_vectors[:, QUERY_RANK:]
    scale = (PLAIN_HEAD_SIZE + ROTARY_SIZE) ** (-0.5)

    def absorb(carry, keys, values):
        row_max, row_total, accum = carry
        scores = (
            jnp.einsum("qhd,khd->hqk", query_vectors, keys, preferred_element_type=jnp.float32)
            * scale
        )
        new_max = jnp.maximum(row_max, jnp.max(scores, axis=-1))
        factor = jnp.exp(row_max - new_max)
        exp_scores = jnp.exp(scores - new_max[:, :, None])
        row_total = row_total * factor + jnp.sum(exp_scores, axis=-1)
        summed = jnp.einsum(
            "hqk,khd->qhd",
            exp_scores.astype(jnp.bfloat16),
            values,
            preferred_element_type=jnp.float32,
        )
        accum = accum * jnp.transpose(factor)[:, :, None] + summed
        return (new_max, row_total, accum)

    initial = (
        jnp.full((local_heads, rows), -1e30, jnp.float32),
        jnp.zeros((local_heads, rows), jnp.float32),
        jnp.zeros((rows, local_heads, VALUE_HEAD_SIZE), jnp.float32),
    )
    key_width = local_heads * (PLAIN_HEAD_SIZE + ROTARY_SIZE)
    total_count = key_value_rows.shape[0]
    key_value_pair = jnp.dot(
        key_value_rows[:, :KEY_VALUE_RANK], key_value_up_weight, preferred_element_type=jnp.float32
    ).reshape(total_count, local_heads, PLAIN_HEAD_SIZE + VALUE_HEAD_SIZE)
    shared = jnp.broadcast_to(
        key_value_rows[:, None, KEY_VALUE_RANK:].astype(jnp.float32),
        (total_count, local_heads, ROTARY_SIZE),
    )
    keys = jnp.concatenate([key_value_pair[..., :PLAIN_HEAD_SIZE], shared], axis=-1)
    keys = rotate_tail(norm_rows(keys, key_gain), positions).astype(jnp.bfloat16)
    own_keys = keys
    own_values = key_value_pair[..., PLAIN_HEAD_SIZE:].astype(jnp.bfloat16)
    key_block = jnp.concatenate(
        [
            own_keys.reshape(rows, key_width),
            own_values.reshape(rows, local_heads * VALUE_HEAD_SIZE),
        ],
        axis=1,
    )

    def take_heads(carry, block):
        keys = block[:, :key_width].reshape(rows, local_heads, PLAIN_HEAD_SIZE + ROTARY_SIZE)
        values = block[:, key_width:].reshape(rows, local_heads, VALUE_HEAD_SIZE)
        return absorb(carry, keys, values)

    carry = initial
    piece = lax.all_gather(key_block, "sp", axis=0, tiled=True)
    total_count = piece.shape[0] // rows
    stacked = piece.reshape((total_count, rows) + piece.shape[1:])

    def one_block(carry_in, pair):
        block, number = pair
        return (take_heads(carry_in, block), None)

    carry, unused = lax.scan(one_block, carry, (stacked, jnp.arange(total_count, dtype=jnp.int32)))
    row_max, row_total, accum = carry
    attention = (
        (accum / jnp.transpose(row_total)[:, :, None])
        .astype(jnp.bfloat16)
        .reshape(rows, local_heads * VALUE_HEAD_SIZE)
    )
    row_logsum = row_max + jnp.log(row_total)
    padded = with_halo(pool_input, (("sp", 0),), rim_width)
    running = jnp.concatenate(
        [jnp.zeros((1, pool_cols), jnp.float32), jnp.cumsum(padded.astype(jnp.float32), axis=0)],
        axis=0,
    )
    length = rows * sp_count
    group = lax.axis_index("tp") * groups_here + 0
    half = jnp.left_shift(jnp.int32(1), group % 4)
    upper_sum = lax.dynamic_slice_in_dim(running, rim_width + half, rows, 0)
    lower_sum = lax.dynamic_slice_in_dim(running, rim_width - half, rows, 0)
    total_count = (jnp.minimum(places + half, length) - jnp.maximum(places - half, 0)).astype(
        jnp.float32
    )[:, None]
    pooled = ((upper_sum - lower_sum) / total_count - pool_input.astype(jnp.float32)).astype(
        jnp.bfloat16
    )
    mapped = jnp.dot(pooled, w_pool_mix[0], preferred_element_type=jnp.float32)
    pieces = (mapped * pool_scale.astype(jnp.float32)).astype(jnp.bfloat16)
    mixed = sent_and_summed(
        (
            jnp.dot(attention, w_out_attn, preferred_element_type=jnp.float32)
            + jnp.dot(pieces, w_out_pool, preferred_element_type=jnp.float32)
        ).astype(jnp.bfloat16),
        "tp",
        0,
    ).astype(jnp.bfloat16)
    return (mixed, row_logsum)


def solution(mesh):
    placed = (
        P(("sp", "tp"), None),
        P(),
        P(),
        P(),
        P(),
        P(),
        P(),
        P(),
        P(None, "tp"),
        P(None, "tp"),
        P(),
        P(),
        P("tp", None, None),
        P("tp"),
        P("tp", None),
        P("tp", None),
    )
    return jax.shard_map(
        shards,
        mesh=mesh,
        in_specs=placed,
        out_specs=(P(("sp", "tp"), None), P("tp", "sp")),
        check_vma=False,
    )
```

profile of v0, /device:TPU:1, one launch (start us, length us, event | category | flops | bytes accessed | tf_op | source)
XLA Modules:
  0.0 293.6 jit_solution(1877036699857983679)
XLA Ops:
  7.2 2.4 broadcast_in_dim.13
  9.6 7.5 %all-to-all-start = ((bf16[8,48,2048]{2,1,0:T(8,128)(2,1)}), bf16[8,48,2048]{2,1,0:T(8,128)(2,1)}, u32[]{:S(2)}, u32[]{:S(2)}) async-start(bf16[8,48,2048]{2,1,0:T(8,128)(2,1)} %broadcast_in_dim.13), calls=%async_computation | async-start | bytes 3145728 | tf_op jit(solution)/shard_map/all_to_all | solution.py:21
  17.4 20.4 %all-to-all-done = bf16[8,48,2048]{2,1,0:T(8,128)(2,1)} async-done(((bf16[8,48,2048]{2,1,0:T(8,128)(2,1)}), bf16[8,48,2048]{2,1,0:T(8,128)(2,1)}, u32[]{:S(2)}, u32[]{:S(2)}) %all-to-all-start) | async-done | bytes 1572896 | tf_op jit(solution)/shard_map/all_to_all | solution.py:21
  37.8 1.8 multiply_reduce_fusion
  39.7 1.9 fusion.11
  44.0 1.1 multiply_reduce_fusion.1
  46.9 2.4 convolution_convert_fusion
  49.4 1.7 collective-permute-start
  51.0 1.3 collective-permute-start.1
  52.4 3.1 %collective-permute-done.1 = bf16[8,64]{0,1:T(8,128)(2,1)S(1)} collective-permute-done((bf16[8,64]{0,1:T(8,128)(2,1)S(1)}, bf16[8,64]{0,1:T(8,128)(2,1)S(1)}, u32[]{:S(2)}, u32[]{:S(2)}) %collective-permute-start.1) | collective-permute-done | bytes 1056 | tf_op jit(solution)/shard_map/ppermute | solution.py:43
  55.6 1.2 reduce-window.6
  57.2 2.5 fusion.13
  59.8 104.6 %all-gather.2.cloned.1.call-done = bf16[12288,480]{0,1:T(8,128)(2,1)} async-done(((bf16[384,480]{0,1:T(8,128)(2,1)}), bf16[12288,480]{0,1:T(8,128)(2,1)}) %all-gather.2.cloned.1.call-update) | async-done | bytes 11796496 | tf_op jit(solution)/shard_map/all_gather | solution.py:204
  164.4 10.2 %copy.36 = bf16[60,32,8,384]{3,2,0,1:T(8,128)(2,1)} copy(bf16[60,32,8,384]{3,2,1,0:T(8,128)(2,1)} %bitcast.96) | data formatting | bytes 23592960 | tf_op jit(solution)/shard_map/reshape | solution.py:206
  174.6 77.1 %while.15 = (s32[]{:T(128)}, f32[3,384]{1,0:T(4,128)S(1)}, f32[3,384]{1,0:T(4,128)S(1)}, f32[384,3,64]{0,2,1:T(8,128)S(1)}, bf16[32,384,480]{1,2,0:T(8,128)(2,1)...) while((s32[]{:T(128)}, f32[3,384]{1,0:T(4,128)S(1)}, f32[3,384]{1,0:T(4,128)S(1)}, ...), condition=%wide.region_8.9_spmd.clone, body=%wide.region_5.8_spmd.clone.sunk | while | flops 145324800 | bytes 8036461 | solution.py:212
  174.6 1.1 dynamic-slice_bitcast_fusion.2
  177.0 1.0 dynamic-slice_bitcast_fusion.2
  179.4 1.0 dynamic-slice_bitcast_fusion.2
  181.9 1.0 dynamic-slice_bitcast_fusion.2
  184.3 1.0 dynamic-slice_bitcast_fusion.2
  186.7 1.0 dynamic-slice_bitcast_fusion.2
  189.1 1.0 dynamic-slice_bitcast_fusion.2
  191.5 1.0 dynamic-slice_bitcast_fusion.2
  193.9 1.0 dynamic-slice_bitcast_fusion.2
  196.3 1.0 dynamic-slice_bitcast_fusion.2
  198.7 1.0 dynamic-slice_bitcast_fusion.2
  201.1 1.0 dynamic-slice_bitcast_fusion.2
  203.5 1.0 dynamic-slice_bitcast_fusion.2
  205.9 1.0 dynamic-slice_bitcast_fusion.2
  208.3 1.0 dynamic-slice_bitcast_fusion.2
  213.2 1.0 dynamic-slice_bitcast_fusion.2
  215.6 1.0 dynamic-slice_bitcast_fusion.2
  218.0 1.0 dynamic-slice_bitcast_fusion.2
  220.4 1.0 dynamic-slice_bitcast_fusion.2
  222.8 1.0 dynamic-slice_bitcast_fusion.2
  225.2 1.0 dynamic-slice_bitcast_fusion.2
  227.6 1.0 dynamic-slice_bitcast_fusion.2
  230.0 1.0 dynamic-slice_bitcast_fusion.2
  232.4 1.0 dynamic-slice_bitcast_fusion.2
  234.8 1.0 dynamic-slice_bitcast_fusion.2
  237.2 1.0 dynamic-slice_bitcast_fusion.2
  239.7 1.0 dynamic-slice_bitcast_fusion.2
  242.1 1.0 dynamic-slice_bitcast_fusion.2
  244.5 1.0 dynamic-slice_bitcast_fusion.2
  251.7 3.7 %add_convert_fusion = bf16[384,2048]{1,0:T(8,128)(2,1)} fusion(f32[384,2048]{1,0:T(8,128)} %fusion.13, bf16[384,192]{0,1:T(8,128)(2,1)S(1)} %bitcast.103, bf16[192,2048]{1,0:T(8,128)(2,1)S(1)} %copy-done.3), kind=kOutput, calls=%fused_computation.21 | convolution fusion | flops 303562752 | bytes 5652480 | tf_op jit(solution)/shard_map/dot_general | solution.py:240
  255.4 8.2 %all-to-all-start.1 = ((bf16[8,48,2048]{2,1,0:T(8,128)(2,1)}), bf16[8,48,2048]{2,1,0:T(8,128)(2,1)}, u32[]{:S(2)}, u32[]{:S(2)}) async-start(bf16[8,48,2048]{2,1,0:T(8,128)(2,1)} %bitcast.97), calls=%async_computation.1 | async-start | bytes 3145728 | tf_op jit(solution)/shard_map/all_to_all | solution.py:56
  264.3 20.1 %all-to-all-done.1 = bf16[8,48,2048]{2,1,0:T(8,128)(2,1)} async-done(((bf16[8,48,2048]{2,1,0:T(8,128)(2,1)}), bf16[8,48,2048]{2,1,0:T(8,128)(2,1)}, u32[]{:S(2)}, u32[]{:S(2)}) %all-to-all-start.1) | async-done | bytes 1572896 | tf_op jit(solution)/shard_map/all_to_all | solution.py:56
  284.3 2.4 reduce_sum.71
  (336 shorter events, 50.7 us)
Async XLA Ops:
  7.2 36.8 %copy-start = (bf16[2048,512]{1,0:T(8,128)(2,1)S(1)}, bf16[2048,512]{1,0:T(8,128)(2,1)}, u32[]{:S(2)}) copy-start(bf16[2048,512]{1,0:T(8,128)(2,1)} %param.20) | copy-start | bytes 6291460
  9.6 7.5 %copy-start.11 = (bf16[96]{0:T(256)(128)(2,1)S(1)}, bf16[96]{0:T(256)(128)(2,1)}, u32[]{:S(2)}) copy-start(bf16[96]{0:T(256)(128)(2,1)} %param.28) | copy-start | bytes 580
  9.6 7.6 %copy-start.12 = (bf16[96]{0:T(256)(128)(2,1)S(1)}, bf16[96]{0:T(256)(128)(2,1)}, u32[]{:S(2)}) copy-start(bf16[96]{0:T(256)(128)(2,1)} %param.29) | copy-start | bytes 580
  9.6 7.6 %copy-start.13 = (bf16[256]{0:T(256)(128)(2,1)S(1)}, bf16[256]{0:T(256)(128)(2,1)}, u32[]{:S(2)}) copy-start(bf16[256]{0:T(256)(128)(2,1)} %param.23) | copy-start | bytes 1540
  9.6 7.6 %copy-start.10 = (bf16[512]{0:T(512)(128)(2,1)S(1)}, bf16[512]{0:T(512)(128)(2,1)}, u32[]{:S(2)}) copy-start(bf16[512]{0:T(512)(128)(2,1)} %param.21) | copy-start | bytes 3076
  9.6 7.6 %copy-start.9 = (bf16[2048]{0:T(1024)(128)(2,1)S(1)}, bf16[2048]{0:T(1024)(128)(2,1)}, u32[]{:S(2)}) copy-start(bf16[2048]{0:T(1024)(128)(2,1)} %param.19) | copy-start | bytes 12292
  9.6 28.2 %all-to-all-start = ((bf16[8,48,2048]{2,1,0:T(8,128)(2,1)}), bf16[8,48,2048]{2,1,0:T(8,128)(2,1)}, u32[]{:S(2)}, u32[]{:S(2)}) async-start(bf16[8,48,2048]{2,1,0:T(8,128)(2,1)} %broadcast_in_dim.13), calls=%async_computation | async-start | bytes 3145728 | tf_op jit(solution)/shard_map/all_to_all | solution.py:21
  17.1 147.2 %all-gather.2.cloned.1.call-start = ((), (), s32[]{:S(2)}) async-start(), calls=%async_computation.2 | async-start | bytes 12165120 | tf_op jit(solution)/shard_map/all_gather | solution.py:204
  39.6 2.0 copy-start.2
  41.7 2.3 copy-start.1
  41.7 1.1 copy-start.6
  42.5 0.9 copy-start.7
  44.0 1.1 copy-start.4
  45.6 1.2 copy-start.14
  46.9 10.3 %copy-start.5 = (bf16[64,2048]{1,0:T(8,128)(2,1)S(1)}, bf16[64,2048]{1,0:T(8,128)(2,1)}, u32[]{:S(2)}) copy-start(bf16[64,2048]{1,0:T(8,128)(2,1)} %param.33) | copy-start | bytes 786436
  46.9 10.3 %copy-start.8 = (bf16[1,64,64]{2,1,0:T(8,128)(2,1)S(1)}, bf16[1,64,64]{2,1,0:T(8,128)(2,1)}, u32[]{:S(2)}) copy-start(bf16[1,64,64]{2,1,0:T(8,128)(2,1)} %param.30) | copy-start | bytes 24580
  49.4 3.0 %collective-permute-start = (bf16[8,64]{0,1:T(8,128)(2,1)S(1)}, bf16[8,64]{0,1:T(8,128)(2,1)S(1)}, u32[]{:S(2)}, u32[]{:S(2)}) collective-permute-start(bf16[8,64]{0,1:T(8,128)(2,1)S(1)} %get-tuple-element.94), channel_id=1, source_target_pairs={{0,8},{8,16},{16,24},{24,32},{32,40},{40,48},{48,56},{56,64},{64,7... | collective-permute-start | bytes 3080 | tf_op jit(solution)/shard_map/ppermute | solution.py:40
  51.0 4.5 %collective-permute-start.1 = (bf16[8,64]{0,1:T(8,128)(2,1)S(1)}, bf16[8,64]{0,1:T(8,128)(2,1)S(1)}, u32[]{:S(2)}, u32[]{:S(2)}) collective-permute-start(bf16[8,64]{0,1:T(8,128)(2,1)S(1)} %get-tuple-element.95), channel_id=1, source_target_pairs={{8,0},{16,8},{24,16},{32,24},{40,32},{48,40},{56,48},{64,56},{72,6... | collective-permute-start | bytes 3080 | tf_op jit(solution)/shard_map/ppermute | solution.py:43
  174.6 77.2 %copy-start.3 = (bf16[192,2048]{1,0:T(8,128)(2,1)S(1)}, bf16[192,2048]{1,0:T(8,128)(2,1)}, u32[]{:S(2)}) copy-start(bf16[192,2048]{1,0:T(8,128)(2,1)} %param.32) | copy-start | bytes 2359300
  255.4 28.9 %all-to-all-start.1 = ((bf16[8,48,2048]{2,1,0:T(8,128)(2,1)}), bf16[8,48,2048]{2,1,0:T(8,128)(2,1)}, u32[]{:S(2)}, u32[]{:S(2)}) async-start(bf16[8,48,2048]{2,1,0:T(8,128)(2,1)} %bitcast.97), calls=%async_computation.1 | async-start | bytes 3145728 | tf_op jit(solution)/shard_map/all_to_all | solution.py:56
Sparse Core Ops, SparseCore 0:
  46.9 117.4 all-gather.1
where the time goes:
time: 295 us; the launch traced here: 294 us
  waiting for transfers between devices  148 us (50%)
  local copies, waits for them, and re-layouts  48.1 us (16%)
  matrix products  41.6 us (14%)
  other arithmetic  20.5 us (7%)
  starting transfers between devices  18.7 us (6%)
  between operations  14.5 us (5%)
    all_gather x1, waiting for transfers between devices, shards(): piece = lax.all_gather(key_block, 'sp', axis=0, tiled=True)  105 us
    squeeze x32, local copies, waits for them, and re-layouts, shards(): lax.scan(one_block, carry, (stacked, jnp.arange(total_count, dtype=jnp.in...  33.1 us
    all_to_all x1, waiting for transfers between devices, from_everyone(): lax.all_to_all(jnp.broadcast_to(x[None], (count, *x.shape)), axis, 0, 0,...  20.4 us
    all_to_all x1, waiting for transfers between devices, sent_and_summed(): pieces = lax.all_to_all(cut_along(x, dim, count), axis, 0, 0, tiled=True)  20.1 us
    dot_general x32, matrix products, absorb(): jnp.einsum('qhd,khd->hqk', query_vectors, keys, preferred_element_type=jn...  15.2 us
    dot_general x32, matrix products, absorb(): jnp.einsum('hqk,khd->qhd', exp_scores.astype(jnp.bfloat16), values, prefe...  14.6 us
    reshape x1, local copies, waits for them, and re-layouts, shards(): stacked = piece.reshape((total_count, rows) + piece.shape[1:])  10.2 us
    reduce_sum x32, other arithmetic, absorb(): row_total = row_total * factor + jnp.sum(exp_scores, axis=-1)  9.9 us
  transfers between devices with their start and end apart: 5, of which 4 were waited for; matrix products, arithmetic and copies ran while one was open for 3% of the time, Pallas kernels for 0%

commit v1 on v0

v1 whole, which is shorter than its diff:
```python
import numpy as np

import jax
import jax.numpy as jnp
from jax import lax
from jax.experimental import pallas as pl
from jax.experimental.pallas import tpu as pltpu
from jax.sharding import PartitionSpec as P

MESH = pl.DeviceIdType.MESH
BF, F32 = jnp.bfloat16, jnp.float32
H = 3
TB = 384
OWN = 48
NB = 32
LH = 160
PER = 4
STEPS = NB // PER
EPS = 1e-6
LOG2E = 1.4426950408889634
LN2 = 0.6931471805599453
LENGTH = NB * TB

ROW_ORDER = (0, -1, 1, -2, 2, -3, 3, 4)
X_TARGETS = ((0, 1), (0, -1), (0, 2))


def slot_of(dz, dx):
    dz = (dz + 3) % 8 - 3
    return 4 * ROW_ORDER.index(dz) + dx % 4


def forwards(core, dz, dx):
    if core == 0:
        if dz == 0:
            return (X_TARGETS if dx == 0 else ()) + ((1, 0), (-1, 0))
        if dz in (-1, -2) or (dz == -3 and dx in (0, 1)):
            return ((1, 0),)
        if dz in (1, 2) or (dz == 3 and dx in (2, 3)):
            return ((-1, 0),)
        return ()
    if dx:
        return ()
    if dz == 0:
        return ((1, 0), (-1, 0)) + X_TARGETS
    along = ((1, 0),) if dz in (-1, -2, -3) else ((-1, 0),) if dz in (1, 2) else ()
    return along + X_TARGETS


PLAN = tuple(
    {
        slot_of(dz, dx): tuple((az, ax, slot_of(dz - az, dx - ax)) for az, ax in forwards(core, dz, dx))
        for dz in ROW_ORDER
        for dx in range(4)
    }
    for core in (0, 1)
)
SERVICE = (
    tuple(tuple(range(4 * (p // 3), 4 * (p // 3) + 4)) if p % 3 == 0 else () for p in range(3 * STEPS)),
    tuple(tuple(range(4 * (p // 3), 4 * (p // 3) + 4)) if p % 3 == 0 else () for p in range(3 * STEPS)),
)


def dot(a, b, dims):
    return lax.dot_general(a, b, (dims, ((), ())), preferred_element_type=F32)


def remote(src, dst, send, recv, device):
    return pltpu.make_async_remote_copy(
        src_ref=src, dst_ref=dst, send_sem=send, recv_sem=recv, device_id=device, device_id_type=MESH
    )


def norm_rows(v, gain):
    return v * lax.rsqrt(jnp.mean(v * v, axis=-1, keepdims=True) + EPS) * gain


def column(row, count):
    n = row.shape[1]
    row = jnp.concatenate([row, jnp.zeros((1, 128 - n), F32)], axis=1)
    return jnp.tile(jnp.transpose(jnp.broadcast_to(row, (128, 128)))[:n], (1, count))


def prep(lat, w_ref, k_ref, v_ref, first):
    n = lat.shape[1]
    cols = slice(first, first + n)
    kv = dot(w_ref[...], lat[:256], ((1,), (0,)))
    rope = lat[256:288].astype(F32)
    rho = lat[288:304].astype(F32)
    rho = rho[0:1] + rho[1:2]
    for h in range(H):
        k = kv[h * 64 : (h + 1) * 64]
        r = lax.rsqrt((jnp.sum(k * k, axis=0, keepdims=True) + rho) * (1.0 / 96) + EPS)
        k_ref[h, 0:64, cols] = (k * r).astype(BF)
        k_ref[h, 64:96, cols] = (rope * r).astype(BF)
        v_ref[h, 0:64, cols] = kv[192 + h * 64 : 256 + h * 64].astype(BF)


def soften(h, s, m_ref, acc, v_ref):
    m_old = m_ref[h]
    m_new = jnp.maximum(m_old, jnp.broadcast_to(jnp.max(s, axis=1, keepdims=True), m_old.shape))
    m_ref[h] = m_new
    p = jnp.exp2(s - jnp.tile(m_new, (1, s.shape[1] // 128))).astype(BF)
    acc[h] = acc[h] * jnp.exp2(m_old - m_new) + dot(p, v_ref[h], ((1,), (1,)))


def layer(
    tok, h_wq, h_wkv, h_wr, h_wp, n_gain, q_gain, kv_gain, wq_up, wkv_up, hq_gain, hk_gain, tables,
    w_mix, p_scale, h_woa, h_wop,
    out, lse_out,
    w_q, w_kv, w_r, w_p, w_o, kvg, qg, psend, pool, halo, lat, qs, wup, k_ref, v_ref, m_ref, acc,
    pool_out, cat, pair_s, pair_r, own, row_s, row_r,
    w_sem, g_sem, lat_send, lat_recv, pair_recv, t_sem,
):
    sp, tp = lax.axis_index("sp"), lax.axis_index("tp")
    z, x = lax.div(sp, 4), lax.rem(sp, 4)
    y, c = lax.div(tp, 2), lax.rem(tp, 2)
    partner = tp + 1 - 2 * c

    def chip(az, ax):
        return lax.rem(z + az + 8, 8) * 4 + lax.rem(x + ax + 4, 4)

    weights = [
        pltpu.make_async_copy(a, b, w_sem.at[i])
        for i, (a, b) in enumerate(
            (
                (h_wkv, w_kv),
                (h_wr, w_r),
                (h_wq, w_q),
                (h_wp, w_p),
                (h_woa, w_o.at[pl.ds(0, 192)]),
                (h_wop, w_o.at[pl.ds(192, 64)]),
            )
        )
    ]
    for copy in weights:
        copy.start()

    barrier = pltpu.get_barrier_semaphore()
    friends = [(sp, lax.rem(tp + k, 8)) for k in range(1, 8)]
    friends += [(chip(az, ax), tp) for az, ax in X_TARGETS + ((1, 0), (-1, 0))]
    friends += [(lax.rem(sp + 1, NB), tp), (lax.rem(sp + NB - 1, NB), tp)]
    for friend in friends:
        pl.semaphore_signal(barrier, inc=1, device_id=friend, device_id_type=MESH)

    normed = norm_rows(tok[...].astype(F32), n_gain[...].astype(F32)).astype(BF)
    weights[0].wait()
    weights[1].wait()
    kv = norm_rows(dot(normed, w_kv[...], ((1,), (0,))), kv_gain[...].astype(F32))
    rope = dot(normed, w_r[...], ((1,), (0,)))
    kvg[tp] = jnp.concatenate([kv, rope, jnp.zeros((OWN, 96), F32)], axis=1).astype(BF)
    pl.semaphore_wait(barrier, len(friends))

    def spread(src, dst, kind):
        copies = []
        for k in (4, 3, 5, 2, 6, 1, 7):
            peer = lax.rem(tp + k, 8)
            copies.append(remote(src(peer), dst.at[tp], g_sem.at[kind, k], g_sem.at[kind + 1, 8 - k], (sp, peer)))
            copies[-1].start()
        return copies

    def gathered(dst, kind):
        for k in range(1, 8):
            peer = lax.rem(tp + k, 8)
            remote(dst.at[peer], dst.at[peer], g_sem.at[kind, k], g_sem.at[kind + 1, k], (sp, peer)).wait_recv()

    gathers = spread(lambda peer: kvg.at[tp], kvg, 0)
    weights[2].wait()
    qg[tp] = norm_rows(dot(normed, w_q[...], ((1,), (0,))), q_gain[...].astype(F32)).astype(BF)
    gathers += spread(lambda peer: qg.at[tp], qg, 2)
    weights[3].wait()
    pooled_in = dot(normed, w_p[...], ((1,), (0,))).astype(BF)
    for g in range(8):
        psend[g] = jnp.concatenate([pooled_in[:, g * 64 : (g + 1) * 64], jnp.zeros((OWN, 64), BF)], axis=1)
    pool[tp] = psend[tp]
    gathers += spread(lambda peer: psend.at[peer], pool, 4)

    up = jnp.transpose(wkv_up[...].astype(F32))
    for h in range(H):
        wup[h * 64 : (h + 1) * 64] = up[h * 128 : h * 128 + 64].astype(BF)
        wup[192 + h * 64 : 256 + h * 64] = up[h * 128 + 64 : h * 128 + 128].astype(BF)
    lanes = lax.broadcasted_iota(jnp.int32, (16, TB), 1)
    off_c = jnp.sum(jnp.where(lanes == sp, tables[2], 0.0), axis=1, keepdims=True)
    off_s = jnp.sum(jnp.where(lanes == sp, tables[3], 0.0), axis=1, keepdims=True)
    cosine = tables[0] * off_c - tables[1] * off_s
    sine = tables[1] * off_c + tables[0] * off_s
    kcol = column(hk_gain[...].astype(F32), 3)
    qcol = column(hq_gain[...].astype(F32), 3)
    m_ref[...] = jnp.full(m_ref.shape, -1e30, F32)
    acc[...] = jnp.zeros(acc.shape, F32)
    k_ref[...] = jnp.zeros(k_ref.shape, BF)
    v_ref[...] = jnp.zeros(v_ref.shape, BF)
    v_ref[:, 64:80, :] = jnp.ones((H, 16, v_ref.shape[2]), BF)

    gathered(kvg, 0)
    turned = jnp.transpose(kvg[...].reshape(TB, TB).astype(F32))
    rope = turned[256:288]
    rho = jnp.sum(rope * rope, axis=0, keepdims=True)
    rho_hi = rho.astype(BF).astype(F32)
    rope = rope * kcol[64:96]
    first, second = rope[:16], rope[16:]
    row = lax.broadcasted_iota(jnp.int32, (32, TB), 0)
    last = jnp.where(row == 0, rho_hi, jnp.where(row == 1, rho - rho_hi, 0.0))
    lat[0, 0] = turned[:LH].astype(BF)
    lat[0, 1] = jnp.concatenate(
        [turned[LH:256], first * cosine - second * sine, first * sine + second * cosine, last], axis=0
    ).astype(BF)

    def outgoing(core, s):
        copies = [
            remote(lat.at[s, core], lat.at[t, core], lat_send.at[s, k], lat_recv.at[t], (chip(az, ax), tp))
            for k, (az, ax, t) in enumerate(PLAN[core][s])
        ]
        if s:
            copies.append(
                remote(lat.at[s, core], lat.at[s, core], lat_send.at[s, 5], pair_recv.at[s], (sp, partner))
            )
        return copies

    def serve(point):
        for core in (0, 1):
            slots = SERVICE[core][point]
            if slots:

                @pl.when(c == core)
                def _():
                    for s in slots:
                        if s:
                            remote(
                                lat.at[s, core], lat.at[s, core], lat_send.at[s, 0], lat_recv.at[s], (sp, partner)
                            ).wait_recv()
                        for copy in outgoing(core, s):
                            copy.start()

    for core in (0, 1):

        @pl.when(c == core)
        def _():
            for copy in outgoing(core, 0):
                copy.start()

    gathered(pool, 4)
    halos = [
        remote(
            pool.at[7, pl.ds(32, 16)], halo.at[0], t_sem.at[0, 0], t_sem.at[1, 0], (lax.rem(sp + 1, NB), tp)
        ),
        remote(
            pool.at[0, pl.ds(0, 16)], halo.at[1], t_sem.at[0, 1], t_sem.at[1, 1], (lax.rem(sp + NB - 1, NB), tp)
        ),
    ]
    for copy in halos:
        copy.start()

    gathered(qg, 2)
    qt = dot(wq_up[...], qg[...].reshape(TB, 512), ((0,), (1,)))
    scale = 96.0 ** -0.5 * LOG2E
    for h in range(H):
        q = qt[h * 96 : (h + 1) * 96]
        q = q * (lax.rsqrt(jnp.mean(q * q, axis=0, keepdims=True) + EPS) * scale) * qcol
        first, second = q[64:80], q[80:96]
        q = jnp.concatenate(
            [
                q[:64] * kcol[:64],
                first * cosine - second * sine,
                first * sine + second * cosine,
                jnp.zeros((32, TB), F32),
            ],
            axis=0,
        )
        qs[h] = jnp.transpose(q).astype(BF)

    for copy in halos:
        copy.wait_recv()
    mine = pool[...].reshape(TB, 128)
    wide = jnp.concatenate([halo[0], mine, halo[1], jnp.zeros((96, 128), BF)], axis=0)
    half = jnp.left_shift(jnp.int32(1), lax.rem(tp, 4))
    here = lax.broadcasted_iota(jnp.int32, (TB, 512), 0)
    there = lax.broadcasted_iota(jnp.int32, (TB, 512), 1) - 16
    place = there + sp * TB
    band = (there >= here - half) & (there < here + half) & (place >= 0) & (place < LENGTH)
    summed = dot(jnp.where(band, 1.0, 0.0).astype(BF), wide, ((1,), (0,)))
    place = lax.broadcasted_iota(jnp.int32, (TB, 128), 0) + sp * TB
    count = jnp.minimum(place + half, LENGTH) - jnp.maximum(place - half, 0)
    pooled = (summed / count.astype(F32) - mine.astype(F32)).astype(BF)
    mapped = dot(pooled[:, :64], w_mix[0], ((1,), (0,)))
    pool_out[...] = (mapped * p_scale[...].astype(F32)).astype(BF)

    def step(i, carry):
        for k in range(STEPS):

            @pl.when(i == k)
            def _():
                if k:
                    serve(3 * k)
                else:
                    for core in (0, 1):

                        @pl.when(c == core)
                        def _():
                            for s in SERVICE[core][0]:
                                if s:
                                    remote(
                                        lat.at[s, core],
                                        lat.at[s, core],
                                        lat_send.at[s, 0],
                                        lat_recv.at[s],
                                        (sp, partner),
                                    ).wait_recv()
                                    for copy in outgoing(core, s):
                                        copy.start()

                for s in range(PER * k, PER * k + PER):
                    if s:
                        remote(
                            lat.at[s, 1 - c], lat.at[s, 1 - c], lat_send.at[s, 5], pair_recv.at[s], (sp, partner)
                        ).wait_recv()

        for j in range(PER):
            prep(lat[i * PER + j].reshape(2 * LH, TB), wup, k_ref, v_ref, j * TB)
        held = None
        for h in range(H):
            s = dot(qs[h], k_ref[h], ((1,), (0,)))
            if held is not None:
                soften(h - 1, held, m_ref, acc, v_ref)
            held = s
            if h < H - 1:
                for k in range(STEPS):
                    if any(SERVICE[core][3 * k + h + 1] for core in (0, 1)):

                        @pl.when(i == k)
                        def _():
                            serve(3 * k + h + 1)

        soften(H - 1, held, m_ref, acc, v_ref)
        return carry

    lax.fori_loop(0, STEPS, step, 0)

    lane = lax.broadcasted_iota(jnp.int32, (TB, 128), 1)
    parts, logs = [], jnp.zeros((TB, 128), F32)
    for h in range(H):
        o = acc[h]
        total = o[:, 64:65]
        parts.append((o[:, :64] / total).astype(BF))
        logs = jnp.where(lane == h, m_ref[h] * LN2 + jnp.log(total), logs)
    lse_out[...] = jnp.transpose(logs)[:H]
    cat[...] = jnp.concatenate(parts + [pool_out[...]], axis=1).reshape(8, OWN, 256)
    weights[4].wait()
    weights[5].wait()

    def rows_of(core):
        return jnp.concatenate([cat[2 * k + core] for k in range(4)], axis=0)

    pair_s[...] = dot(rows_of(1 - c), w_o[...], ((1,), (0,))).astype(BF).reshape(4, OWN, 2048)
    tails = []
    for k in (2, 1, 3, 0):
        there = lax.rem(y + k, 4)
        tails.append(
            remote(pair_s.at[there], pair_r.at[there], t_sem.at[2, k], t_sem.at[3, k], (sp, partner))
        )
        tails[-1].start()
    own[...] = dot(rows_of(c), w_o[...], ((1,), (0,))).reshape(4, OWN, 2048)
    sums = None
    for i, k in enumerate((2, 1, 3, 0)):
        there = lax.rem(y + k, 4)
        tails[i].wait_recv()
        value = own[there] + pair_r[there].astype(F32)
        if k:
            row_s[k - 1] = value.astype(BF)
            copy = remote(
                row_s.at[k - 1], row_r.at[3 - k], t_sem.at[4, k], t_sem.at[5, 4 - k], (sp, 2 * there + c)
            )
            copy.start()
            tails.append(copy)
        else:
            sums = value
    for k in (1, 3, 2):
        remote(row_s.at[k - 1], row_r.at[k - 1], t_sem.at[4, k], t_sem.at[5, k], (sp, partner)).wait_recv()
        sums = sums + row_r[k - 1].astype(F32)
    out[...] = sums.astype(BF)

    for copy in gathers + halos + tails:
        copy.wait_send()
    for core in (0, 1):

        @pl.when(c == core)
        def _():
            for s in range(NB):
                for copy in outgoing(core, s):
                    copy.wait_send()


def rotation_tables():
    half = 16
    freqs = 10000.0 ** (-np.arange(half, dtype=np.float64) / half)
    inside = freqs[:, None] * np.arange(TB)[None, :]
    blocks = np.zeros((half, TB))
    blocks[:, :NB] = freqs[:, None] * (TB * np.arange(NB))[None, :]
    return np.stack([np.cos(inside), np.sin(inside), np.cos(blocks), np.sin(blocks)]).astype(np.float32)


def shards(tokens, norm_gain, query_down_weight, query_latent_norm_gain, key_value_down_weight,
           key_value_latent_gain, w_rope_key, w_pool_in, query_up_weight, key_value_up_weight,
           query_gain, key_gain, w_pool_mix, pool_scale, w_out_attn, w_out_pool):
    vmem, anywhere = pl.BlockSpec(memory_space=pltpu.VMEM), pl.BlockSpec(memory_space=pl.ANY)
    dma, n = pltpu.SemaphoreType.DMA, PER * TB
    return pl.pallas_call(
        layer,
        out_shape=(jax.ShapeDtypeStruct((OWN, 2048), BF), jax.ShapeDtypeStruct((H, TB), F32)),
        in_specs=[vmem] + [anywhere] * 4 + [vmem] * 10 + [anywhere] * 2,
        out_specs=(vmem, vmem),
        scratch_shapes=[
            pltpu.VMEM((2048, 512), BF),
            pltpu.VMEM((2048, 256), BF),
            pltpu.VMEM((2048, 32), BF),
            pltpu.VMEM((2048, 512), BF),
            pltpu.VMEM((256, 2048), BF),
            pltpu.VMEM((8, OWN, TB), BF),
            pltpu.VMEM((8, OWN, 512), BF),
            pltpu.VMEM((8, OWN, 128), BF),
            pltpu.VMEM((8, OWN, 128), BF),
            pltpu.VMEM((2, 16, 128), BF),
            pltpu.VMEM((NB, 2, LH, TB), BF),
            pltpu.VMEM((H, TB, 128), BF),
            pltpu.VMEM((H * 128, 256), BF),
            pltpu.VMEM((H, 128, n), BF),
            pltpu.VMEM((H, 128, n), BF),
            pltpu.VMEM((H, TB, 128), F32),
            pltpu.VMEM((H, TB, 128), F32),
            pltpu.VMEM((TB, 64), BF),
            pltpu.VMEM((8, OWN, 256), BF),
            pltpu.VMEM((4, OWN, 2048), BF),
            pltpu.VMEM((4, OWN, 2048), BF),
            pltpu.VMEM((4, OWN, 2048), F32),
            pltpu.VMEM((3, OWN, 2048), BF),
            pltpu.VMEM((3, OWN, 2048), BF),
            dma((6,)),
            dma((6, 8)),
            dma((NB, 6)),
            dma((NB,)),
            dma((NB,)),
            dma((6, 4)),
        ],
        compiler_params=pltpu.CompilerParams(
            collective_id=0, has_side_effects=True, vmem_limit_bytes=60 * 2**20
        ),
        name="layer",
    )(
        tokens, query_down_weight, key_value_down_weight, w_rope_key, w_pool_in,
        norm_gain[None], query_latent_norm_gain[None], key_value_latent_gain[None],
        query_up_weight, key_value_up_weight, query_gain[None], key_gain[None],
        jnp.asarray(rotation_tables()), w_pool_mix, pool_scale[None], w_out_attn, w_out_pool,
    )


def solution(mesh):
    everywhere = P()
    placed = (
        (P(("sp", "tp"), None),)
        + (everywhere,) * 7
        + (P(None, "tp"),) * 2
        + (everywhere,) * 2
        + (P("tp", None, None), P("tp"), P("tp", None), P("tp", None))
    )
    return jax.shard_map(
        shards,
        mesh=mesh,
        in_specs=placed,
        out_specs=(P(("sp", "tp"), None), P("tp", "sp")),
        check_vma=False,
    )
```

time: 295 us -> 114 us (0.39)
  waiting for transfers between devices: 148 us -> 0 us
  Pallas kernels: 0 us -> 103 us
  matrix products: 41.6 us -> 0 us
  local copies, waits for them, and re-layouts: 48.1 us -> 10.5 us
  other arithmetic: 20.5 us -> 0 us
  starting transfers between devices: 18.7 us -> 0 us
  between operations: 14.5 us -> 0.64 us
    all_gather x1 -> x0, waiting for transfers between devices: 105 us -> none  [shards(): piece = lax.all_gather(key_block, 'sp', axis=0, tiled=True)]
    pallas_call x0 -> x1, Pallas kernels: none -> 103 us  [shards(): pl.pallas_call(layer, out_shape=(jax.ShapeDtypeStruct((OWN, 2048), BF), j...]
    dot_general x72 -> x0, matrix products: 41.6 us -> none  [the longest x32 15.2 us: absorb(): jnp.einsum('qhd,khd->hqk', query_vectors, keys, preferred_element_type=jn...]
    all_to_all x2 -> x0, waiting for transfers between devices: 40.5 us -> none  [the longest x1 20.4 us: from_everyone(): lax.all_to_all(jnp.broadcast_to(x[None], (count, *x.shape)), axis, 0, 0,...]
    squeeze x32 -> x0, local copies, waits for them, and re-layouts: 33.1 us -> none  [shards(): lax.scan(one_block, carry, (stacked, jnp.arange(total_count, dtype=jnp.in...]
    all_to_all x2 -> x0, starting transfers between devices: 15.8 us -> none  [the longest x1 8.25 us: sent_and_summed(): pieces = lax.all_to_all(cut_along(x, dim, count), axis, 0, 0, tiled=True)]
    reduce_sum x36 -> x0, other arithmetic: 14.2 us -> none  [the longest x32 9.9 us: absorb(): row_total = row_total * factor + jnp.sum(exp_scores, axis=-1)]
    reshape x1 -> x0, local copies, waits for them, and re-layouts: 10.2 us -> none  [shards(): stacked = piece.reshape((total_count, rows) + piece.shape[1:])]
  transfers between devices with their start and end apart: 5 -> 0, of which waited for: 4 -> 0; matrix products, arithmetic and copies ran while one was open for 3% -> 0% of each run, Pallas kernels for 0% -> 0%
where the time goes in v1:
time: 114 us
  Pallas kernels  103 us (90%)
  local copies, waits for them, and re-layouts  10.5 us (9%)
    pallas_call x1, Pallas kernels, shards(): pl.pallas_call(layer, out_shape=(jax.ShapeDtypeStruct((OWN, 2048), BF), j...  103 us
    unnamed x4, local copies, waits for them, and re-layouts  6.69 us

profile of v1, /device:TPU:1, one launch (start us, length us, event | category | flops | bytes accessed | tf_op | source)
XLA Modules:
  0.0 113.7 jit_solution(13897097144001375983)
XLA Ops:
  0.6 1.2 %broadcast_in_dim.20.kv_gain = bf16[1,256]{1,0:T(2,128)(2,1)} reshape(bf16[256]{0:T(256)(128)(2,1)} %param.22) | data formatting | bytes 1024 | tf_op jit(solution)/shard_map/broadcast_in_dim | solution.py:450
  1.9 1.3 %broadcast_in_dim.19.q_gain = bf16[1,512]{1,0:T(2,128)(2,1)} reshape(bf16[512]{0:T(512)(128)(2,1)} %param.20) | data formatting | bytes 2048 | tf_op jit(solution)/shard_map/broadcast_in_dim | solution.py:450
  3.1 1.3 %broadcast_in_dim.18.n_gain = bf16[1,2048]{1,0:T(2,128)(2,1)} reshape(bf16[2048]{0:T(1024)(128)(2,1)} %param.18) | data formatting | bytes 8192 | tf_op jit(solution)/shard_map/broadcast_in_dim | solution.py:450
  4.4 1.9 %copy.20.wq_up = bf16[512,288]{1,0:T(8,128)(2,1)} copy(bf16[512,288]{0,1:T(8,128)(2,1)} %param.25) | data formatting | bytes 589824 | tf_op args[8]
  6.3 1.9 %copy.19.h_wr = bf16[2048,32]{1,0:T(8,128)(2,1)} copy(bf16[2048,32]{0,1:T(8,128)(2,1)} %param.23) | data formatting | bytes 262144 | tf_op args[6]
  8.2 102.6 %layer.1 = (bf16[48,2048]{1,0:T(8,128)(2,1)}, f32[3,384]{1,0:T(4,128)}) custom-call(bf16[48,2048]{1,0:T(8,128)(2,1)} %tok.1, bf16[2048,512]{1,0:T(8,128)(2,1)} %h_wq.1, bf16[2048,256]{1,0:T(8,128)(2,1)} %h_wkv.1, bf16[2048,32]{1,0:T(8,128)(2,1)} %copy.19.h_wr, bf16[2048,512]{1,0:T(8,128)(2,1)} %h_wp.1, bf16[1,2048]{1,0:T(2,128)(2,1)} %broadcast_in_dim.18.n_gain, ...), custom_call_target="tpu_custom_call" | custom-call | tf_op jit(solution)/shard_map/layer/pallas_call | solution.py:407
  110.8 1.6 %copy.23 = bf16[48,2048]{1,0:T(8,128)(2,1)} copy(bf16[48,2048]{1,0:T(8,128)(2,1)} %get-tuple-element.4) | data formatting | bytes 393216
  112.4 1.3 %copy.24 = f32[3,384]{1,0:T(4,128)} copy(f32[3,384]{1,0:T(4,128)} %get-tuple-element.5) | data formatting | bytes 9216

commit v2 on v1

--- a/solution.py
+++ b/solution.py
@@ -21,43 +21,54 @@
 LN2 = 0.6931471805599453
 LENGTH = NB * TB
 
-ROW_ORDER = (0, -1, 1, -2, 2, -3, 3, 4)
-X_TARGETS = ((0, 1), (0, -1), (0, 2))
+ORDER = (
+    (0, 0), (0, 1), (-1, 0), (1, 0),
+    (2, 0), (0, 3), (-1, 3), (-2, 0),
+    (1, 1), (1, 3), (0, 2), (-1, 1),
+    (2, 3), (-1, 2), (-3, 0), (3, 0),
+    (1, 2), (-2, 1), (2, 1), (-2, 3),
+    (-2, 2), (3, 3), (3, 1), (4, 0),
+    (-3, 3), (-3, 1), (2, 2), (4, 3),
+    (-3, 2), (4, 2), (4, 1), (3, 2),
+)
+NEAR = ((1, 0), (-1, 0), (0, 1), (0, -1))
 
 
 def slot_of(dz, dx):
-    dz = (dz + 3) % 8 - 3
-    return 4 * ROW_ORDER.index(dz) + dx % 4
+    return ORDER.index(((dz + 3) % 8 - 3, dx % 4))
 
 
 def forwards(core, dz, dx):
     if core == 0:
         if dz == 0:
-            return (X_TARGETS if dx == 0 else ()) + ((1, 0), (-1, 0))
+            return {0: NEAR, 3: ((0, 1), (1, 0), (-1, 0))}.get(dx, ((1, 0), (-1, 0)))
         if dz in (-1, -2) or (dz == -3 and dx in (0, 1)):
             return ((1, 0),)
         if dz in (1, 2) or (dz == 3 and dx in (2, 3)):
             return ((-1, 0),)
         return ()
-    if dx:
-        return ()
-    if dz == 0:
-        return ((1, 0), (-1, 0)) + X_TARGETS
-    along = ((1, 0),) if dz in (-1, -2, -3) else ((-1, 0),) if dz in (1, 2) else ()
-    return along + X_TARGETS
+    if dx == 0:
+        if dz == 0:
+            return NEAR
+        along = ((1, 0),) if dz in (-1, -2, -3) else ((-1, 0),) if dz in (1, 2) else ()
+        return along + ((0, 1), (0, -1))
+    if dx == (3 if dz % 2 == 0 else 1):
+        return ((0, 1 if dx == 3 else -1),)
+    return ()
 
 
 PLAN = tuple(
     {
         slot_of(dz, dx): tuple((az, ax, slot_of(dz - az, dx - ax)) for az, ax in forwards(core, dz, dx))
-        for dz in ROW_ORDER
-        for dx in range(4)
+        for dz, dx in ORDER
     }
     for core in (0, 1)
 )
 SERVICE = (
-    tuple(tuple(range(4 * (p // 3), 4 * (p // 3) + 4)) if p % 3 == 0 else () for p in range(3 * STEPS)),
-    tuple(tuple(range(4 * (p // 3), 4 * (p // 3) + 4)) if p % 3 == 0 else () for p in range(3 * STEPS)),
+    ((2, 3, 5, 1), (), (), (7, 4, 10, 6, 9), (), (11, 8), (), (14, 15), (13, 16), (19, 12), (), (18,), (17,),
+     (26, 23), (21,), (20, 22), (24,), (25, 31), (27,), (28,), (), (30, 29), (), ()),
+    ((2, 3, 5, 1), (), (), (11, 7, 4, 6, 8, 9), (10, 13), (19, 17), (14, 15, 12), (18,), (16,), (20,), (25, 24),
+     (23, 22, 21), (), (26,), (), (28, 27), (30,), (31,), (), (29,), (), (), (), ()),
 )
 
 
@@ -73,6 +84,11 @@
 
 def norm_rows(v, gain):
     return v * lax.rsqrt(jnp.mean(v * v, axis=-1, keepdims=True) + EPS) * gain
+
+
+def in_a_row(ref):
+    v = ref[...].astype(F32)
+    return jnp.concatenate([v[i : i + 1] for i in range(v.shape[0])], axis=1)
 
 
 def column(row, count):
@@ -138,16 +154,16 @@
 
     barrier = pltpu.get_barrier_semaphore()
     friends = [(sp, lax.rem(tp + k, 8)) for k in range(1, 8)]
-    friends += [(chip(az, ax), tp) for az, ax in X_TARGETS + ((1, 0), (-1, 0))]
+    friends += [(chip(az, ax), tp) for az, ax in NEAR]
     friends += [(lax.rem(sp + 1, NB), tp), (lax.rem(sp + NB - 1, NB), tp)]
     for friend in friends:
         pl.semaphore_signal(barrier, inc=1, device_id=friend, device_id_type=MESH)
 
-    normed = norm_rows(tok[...].astype(F32), n_gain[...].astype(F32)).astype(BF)
+    normed = norm_rows(tok[...].astype(F32), in_a_row(n_gain)).astype(BF)
     weights[0].wait()
     weights[1].wait()
-    kv = norm_rows(dot(normed, w_kv[...], ((1,), (0,))), kv_gain[...].astype(F32))
-    rope = dot(normed, w_r[...], ((1,), (0,)))
+    kv = norm_rows(dot(normed, w_kv[...], ((1,), (0,))), in_a_row(kv_gain))
+    rope = dot(normed, w_r[...], ((1,), (1,)))
     kvg[tp] = jnp.concatenate([kv, rope, jnp.zeros((OWN, 96), F32)], axis=1).astype(BF)
     pl.semaphore_wait(barrier, len(friends))
 
@@ -166,7 +182,7 @@
 
     gathers = spread(lambda peer: kvg.at[tp], kvg, 0)
     weights[2].wait()
-    qg[tp] = norm_rows(dot(normed, w_q[...], ((1,), (0,))), q_gain[...].astype(F32)).astype(BF)
+    qg[tp] = norm_rows(dot(normed, w_q[...], ((1,), (0,))), in_a_row(q_gain)).astype(BF)
     gathers += spread(lambda peer: qg.at[tp], qg, 2)
     weights[3].wait()
     pooled_in = dot(normed, w_p[...], ((1,), (0,))).astype(BF)
@@ -252,7 +268,7 @@
         copy.start()
 
     gathered(qg, 2)
-    qt = dot(wq_up[...], qg[...].reshape(TB, 512), ((0,), (1,)))
+    qt = dot(wq_up[...], qg[...].reshape(TB, 512), ((1,), (1,)))
     scale = 96.0 ** -0.5 * LOG2E
     for h in range(H):
         q = qt[h * 96 : (h + 1) * 96]
@@ -412,7 +428,7 @@
         scratch_shapes=[
             pltpu.VMEM((2048, 512), BF),
             pltpu.VMEM((2048, 256), BF),
-            pltpu.VMEM((2048, 32), BF),
+            pltpu.VMEM((32, 2048), BF),
             pltpu.VMEM((2048, 512), BF),
             pltpu.VMEM((256, 2048), BF),
             pltpu.VMEM((8, OWN, TB), BF),
@@ -446,9 +462,9 @@
         ),
         name="layer",
     )(
-        tokens, query_down_weight, key_value_down_weight, w_rope_key, w_pool_in,
-        norm_gain[None], query_latent_norm_gain[None], key_value_latent_gain[None],
-        query_up_weight, key_value_up_weight, query_gain[None], key_gain[None],
+        tokens, query_down_weight, key_value_down_weight, w_rope_key.T, w_pool_in,
+        norm_gain.reshape(16, 128), query_latent_norm_gain.reshape(4, 128), key_value_latent_gain.reshape(2, 128),
+        query_up_weight.T, key_value_up_weight, query_gain[None], key_gain[None],
         jnp.asarray(rotation_tables()), w_pool_mix, pool_scale[None], w_out_attn, w_out_pool,
     )
 

time: 114 us -> 77.2 us (0.68)
  Pallas kernels: 103 us -> 73.5 us
  local copies, waits for them, and re-layouts: 10.5 us -> 2.9 us
    pallas_call x1, Pallas kernels: 103 us -> 73.5 us  [shards(): pl.pallas_call(layer, out_shape=(jax.ShapeDtypeStruct((OWN, 2048), BF), j...]
    unnamed x4 -> x2, local copies, waits for them, and re-layouts: 6.69 us -> 2.9 us
    broadcast_in_dim x3 -> x0, local copies, waits for them, and re-layouts: 3.78 us -> none  [the longest x1 1.29 us: shards(): norm_gain[None]]
where the time goes in v2:
time: 77.2 us; the launch traced here: 77 us
  Pallas kernels  73.5 us (95%)
  local copies, waits for them, and re-layouts  2.9 us (4%)
    pallas_call x1, Pallas kernels, shards(): pl.pallas_call(layer, out_shape=(jax.ShapeDtypeStruct((OWN, 2048), BF), j...  73.5 us
    unnamed x2, local copies, waits for them, and re-layouts  2.9 us

profile of v2, /device:TPU:1, one launch (start us, length us, event | category | flops | bytes accessed | tf_op | source)
XLA Modules:
  0.0 77.0 jit_solution(8214363562566567417)
XLA Ops:
  0.6 73.5 %layer.1 = (bf16[48,2048]{1,0:T(8,128)(2,1)}, f32[3,384]{1,0:T(4,128)}) custom-call(bf16[48,2048]{1,0:T(8,128)(2,1)} %tok.1, bf16[2048,512]{1,0:T(8,128)(2,1)} %h_wq.1, bf16[2048,256]{1,0:T(8,128)(2,1)} %h_wkv.1, bf16[32,2048]{1,0:T(8,128)(2,1)} %bitcast.9, bf16[2048,512]{1,0:T(8,128)(2,1)} %h_wp.1, bf16[16,128]{1,0:T(8,128)(2,1)} %bitcast.10, ...), custom_call_target="tpu_custom_call" | custom-call | tf_op jit(solution)/shard_map/layer/pallas_call | solution.py:423
  74.1 1.6 %copy.21 = bf16[48,2048]{1,0:T(8,128)(2,1)} copy(bf16[48,2048]{1,0:T(8,128)(2,1)} %get-tuple-element.4) | data formatting | bytes 393216
  75.7 1.3 %copy.22 = f32[3,384]{1,0:T(4,128)} copy(f32[3,384]{1,0:T(4,128)} %get-tuple-element.5) | data formatting | bytes 9216

commit v3 on v2

--- a/solution.py
+++ b/solution.py
@@ -72,6 +72,9 @@
 )
 
 
+W_STEPS = {4: (0, 1), 7: (2, 3)}
+
+
 def dot(a, b, dims):
     return lax.dot_general(a, b, (dims, ((), ())), preferred_element_type=F32)
 
@@ -125,8 +128,8 @@
     w_mix, p_scale, h_woa, h_wop,
     out, lse_out,
     w_q, w_kv, w_r, w_p, w_o, kvg, qg, psend, pool, halo, lat, qs, wup, k_ref, v_ref, m_ref, acc,
-    pool_out, cat, pair_s, pair_r, own, row_s, row_r,
-    w_sem, g_sem, lat_send, lat_recv, pair_recv, t_sem,
+    pool_out, cat, cat_r,
+    w_sem, g_sem, lat_send, lat_recv, pair_recv, o_send, o_recv, o_pair, t_sem,
 ):
     sp, tp = lax.axis_index("sp"), lax.axis_index("tp")
     z, x = lax.div(sp, 4), lax.rem(sp, 4)
@@ -144,8 +147,8 @@
                 (h_wr, w_r),
                 (h_wq, w_q),
                 (h_wp, w_p),
-                (h_woa, w_o.at[pl.ds(0, 192)]),
-                (h_wop, w_o.at[pl.ds(192, 64)]),
+                (h_woa, w_o.at[c, pl.ds(0, 192)]),
+                (h_wop, w_o.at[c, pl.ds(192, 64)]),
             )
         )
     ]
@@ -167,29 +170,91 @@
     kvg[tp] = jnp.concatenate([kv, rope, jnp.zeros((OWN, 96), F32)], axis=1).astype(BF)
     pl.semaphore_wait(barrier, len(friends))
 
-    def spread(src, dst, kind):
+    def spread(rows, kind):
         copies = []
-        for k in (4, 3, 5, 2, 6, 1, 7):
-            peer = lax.rem(tp + k, 8)
-            copies.append(remote(src(peer), dst.at[tp], g_sem.at[kind, k], g_sem.at[kind + 1, 8 - k], (sp, peer)))
+        for k in (2, 1, 3):
+            peer = 2 * lax.rem(y + k, 4) + c
+            copies.append(remote(rows.at[tp], rows.at[tp], g_sem.at[kind, k], g_sem.at[kind + 1, 4 - k], (sp, peer)))
+        copies.append(remote(rows.at[tp], rows.at[tp], g_sem.at[kind, 4], g_sem.at[kind + 1, 4], (sp, partner)))
+        for copy in copies:
+            copy.start()
+        return copies
+
+    def gathered(rows, kind):
+        copies = []
+        for k in (1, 3, 2):
+            peer = 2 * lax.rem(y + k, 4) + c
+            remote(rows.at[peer], rows.at[peer], g_sem.at[kind, k], g_sem.at[kind + 1, k], (sp, peer)).wait_recv()
+            copies.append(
+                remote(rows.at[peer], rows.at[peer], g_sem.at[kind, 4 + k], g_sem.at[kind + 1, 4 + k], (sp, partner))
+            )
             copies[-1].start()
+        for k in (0, 1, 3, 2):
+            peer = 2 * lax.rem(y + k, 4) + 1 - c
+            remote(
+                rows.at[peer], rows.at[peer], g_sem.at[kind, 4 + k], g_sem.at[kind + 1, 4 + k], (sp, partner)
+            ).wait_recv()
         return copies
 
-    def gathered(dst, kind):
-        for k in range(1, 8):
-            peer = lax.rem(tp + k, 8)
-            remote(dst.at[peer], dst.at[peer], g_sem.at[kind, k], g_sem.at[kind + 1, k], (sp, peer)).wait_recv()
-
-    gathers = spread(lambda peer: kvg.at[tp], kvg, 0)
+    gathers = spread(kvg, 0)
     weights[2].wait()
     qg[tp] = norm_rows(dot(normed, w_q[...], ((1,), (0,))), in_a_row(q_gain)).astype(BF)
-    gathers += spread(lambda peer: qg.at[tp], qg, 2)
+    gathers += spread(qg, 2)
     weights[3].wait()
     pooled_in = dot(normed, w_p[...], ((1,), (0,))).astype(BF)
     for g in range(8):
         psend[g] = jnp.concatenate([pooled_in[:, g * 64 : (g + 1) * 64], jnp.zeros((OWN, 64), BF)], axis=1)
     pool[tp] = psend[tp]
-    gathers += spread(lambda peer: psend.at[peer], pool, 4)
+
+    def exchange(src, dst, kind):
+        copies = []
+        for k in (4, 3, 5, 2, 6, 7, 1):
+            peer = lax.rem(tp + k, 8)
+            copies.append(
+                remote(src.at[peer], dst.at[tp], g_sem.at[kind, k], g_sem.at[kind + 1, 8 - k], (sp, peer))
+            )
+            copies[-1].start()
+        return copies
+
+    def exchanged(dst, kind, k):
+        peer = lax.rem(tp + k, 8)
+        remote(dst.at[peer], dst.at[peer], g_sem.at[kind, k], g_sem.at[kind + 1, k], (sp, peer)).wait_recv()
+
+    gathers += exchange(psend, pool, 4)
+
+    weights[4].wait()
+    weights[5].wait()
+
+    def half_of(shard, part):
+        return w_o.at[shard, pl.ds(128 * part, 128)]
+
+    def around(k, part, i, step):
+        return remote(
+            half_of(2 * k + c, part),
+            half_of(2 * ((k - step) % 4) + c, part),
+            o_send.at[i],
+            o_recv.at[i],
+            (sp, 2 * lax.rem(y + step + 4, 4) + c),
+        )
+
+    def across(k, part):
+        shard = half_of(2 * k + c, part)
+        return remote(shard, shard, o_send.at[6 + 2 * k + part], o_pair.at[2 * k + part], (sp, partner))
+
+    rounds = [around(0, 1, 0, 1), around(0, 0, 1, -1), around(0, 0, 2, 1), around(0, 1, 3, -1)]
+    rounds += [around(3, 1, 4, 1), around(1, 0, 5, -1)]
+    landed = ((3, 1), (1, 0), (3, 0), (1, 1), (2, 1), (2, 0))
+    acrosses = {(k, part): across(k, part) for k in range(4) for part in (0, 1)}
+    for copy in rounds[:4]:
+        copy.start()
+    acrosses[0, 0].start()
+    acrosses[0, 1].start()
+
+    def pass_on(i):
+        rounds[i].wait_recv()
+        if i < 2:
+            rounds[4 + i].start()
+        acrosses[landed[i]].start()
 
     up = jnp.transpose(wkv_up[...].astype(F32))
     for h in range(H):
@@ -208,7 +273,7 @@
     v_ref[...] = jnp.zeros(v_ref.shape, BF)
     v_ref[:, 64:80, :] = jnp.ones((H, 16, v_ref.shape[2]), BF)
 
-    gathered(kvg, 0)
+    gathers += gathered(kvg, 0)
     turned = jnp.transpose(kvg[...].reshape(TB, TB).astype(F32))
     rope = turned[256:288]
     rho = jnp.sum(rope * rope, axis=0, keepdims=True)
@@ -255,19 +320,7 @@
             for copy in outgoing(core, 0):
                 copy.start()
 
-    gathered(pool, 4)
-    halos = [
-        remote(
-            pool.at[7, pl.ds(32, 16)], halo.at[0], t_sem.at[0, 0], t_sem.at[1, 0], (lax.rem(sp + 1, NB), tp)
-        ),
-        remote(
-            pool.at[0, pl.ds(0, 16)], halo.at[1], t_sem.at[0, 1], t_sem.at[1, 1], (lax.rem(sp + NB - 1, NB), tp)
-        ),
-    ]
-    for copy in halos:
-        copy.start()
-
-    gathered(qg, 2)
+    gathers += gathered(qg, 2)
     qt = dot(wq_up[...], qg[...].reshape(TB, 512), ((1,), (1,)))
     scale = 96.0 ** -0.5 * LOG2E
     for h in range(H):
@@ -285,27 +338,45 @@
         )
         qs[h] = jnp.transpose(q).astype(BF)
 
+    for k in range(1, 8):
+        exchanged(pool, 4, k)
+    halos = [
+        remote(
+            pool.at[7, pl.ds(32, 16)], halo.at[0], t_sem.at[0, 0], t_sem.at[1, 0], (lax.rem(sp + 1, NB), tp)
+        ),
+        remote(
+            pool.at[0, pl.ds(0, 16)], halo.at[1], t_sem.at[0, 1], t_sem.at[1, 1], (lax.rem(sp + NB - 1, NB), tp)
+        ),
+    ]
     for copy in halos:
-        copy.wait_recv()
-    mine = pool[...].reshape(TB, 128)
-    wide = jnp.concatenate([halo[0], mine, halo[1], jnp.zeros((96, 128), BF)], axis=0)
-    half = jnp.left_shift(jnp.int32(1), lax.rem(tp, 4))
-    here = lax.broadcasted_iota(jnp.int32, (TB, 512), 0)
-    there = lax.broadcasted_iota(jnp.int32, (TB, 512), 1) - 16
-    place = there + sp * TB
-    band = (there >= here - half) & (there < here + half) & (place >= 0) & (place < LENGTH)
-    summed = dot(jnp.where(band, 1.0, 0.0).astype(BF), wide, ((1,), (0,)))
-    place = lax.broadcasted_iota(jnp.int32, (TB, 128), 0) + sp * TB
-    count = jnp.minimum(place + half, LENGTH) - jnp.maximum(place - half, 0)
-    pooled = (summed / count.astype(F32) - mine.astype(F32)).astype(BF)
-    mapped = dot(pooled[:, :64], w_mix[0], ((1,), (0,)))
-    pool_out[...] = (mapped * p_scale[...].astype(F32)).astype(BF)
+        copy.start()
+
+    def pooling():
+        for copy in halos:
+            copy.wait_recv()
+        mine = pool[...].reshape(TB, 128)
+        wide = jnp.concatenate([halo[0], mine, halo[1], jnp.zeros((96, 128), BF)], axis=0)
+        half = jnp.left_shift(jnp.int32(1), lax.rem(tp, 4))
+        here = lax.broadcasted_iota(jnp.int32, (TB, 512), 0)
+        there = lax.broadcasted_iota(jnp.int32, (TB, 512), 1) - 16
+        place = there + sp * TB
+        band = (there >= here - half) & (there < here + half) & (place >= 0) & (place < LENGTH)
+        summed = dot(jnp.where(band, 1.0, 0.0).astype(BF), wide, ((1,), (0,)))
+        place = lax.broadcasted_iota(jnp.int32, (TB, 128), 0) + sp * TB
+        count = jnp.minimum(place + half, LENGTH) - jnp.maximum(place - half, 0)
+        pooled = (summed / count.astype(F32) - mine.astype(F32)).astype(BF)
+        mapped = dot(pooled[:, :64], w_mix[0], ((1,), (0,)))
+        pool_out[...] = (mapped * p_scale[...].astype(F32)).astype(BF)
 
     def step(i, carry):
         for k in range(STEPS):
 
             @pl.when(i == k)
             def _():
+                if k == 1:
+                    pooling()
+                for i_round in W_STEPS.get(k, ()):
+                    pass_on(i_round)
                 if k:
                     serve(3 * k)
                 else:
@@ -361,41 +432,26 @@
         logs = jnp.where(lane == h, m_ref[h] * LN2 + jnp.log(total), logs)
     lse_out[...] = jnp.transpose(logs)[:H]
     cat[...] = jnp.concatenate(parts + [pool_out[...]], axis=1).reshape(8, OWN, 256)
-    weights[4].wait()
-    weights[5].wait()
-
-    def rows_of(core):
-        return jnp.concatenate([cat[2 * k + core] for k in range(4)], axis=0)
-
-    pair_s[...] = dot(rows_of(1 - c), w_o[...], ((1,), (0,))).astype(BF).reshape(4, OWN, 2048)
-    tails = []
-    for k in (2, 1, 3, 0):
-        there = lax.rem(y + k, 4)
-        tails.append(
-            remote(pair_s.at[there], pair_r.at[there], t_sem.at[2, k], t_sem.at[3, k], (sp, partner))
-        )
-        tails[-1].start()
-    own[...] = dot(rows_of(c), w_o[...], ((1,), (0,))).reshape(4, OWN, 2048)
-    sums = None
-    for i, k in enumerate((2, 1, 3, 0)):
-        there = lax.rem(y + k, 4)
-        tails[i].wait_recv()
-        value = own[there] + pair_r[there].astype(F32)
-        if k:
-            row_s[k - 1] = value.astype(BF)
-            copy = remote(
-                row_s.at[k - 1], row_r.at[3 - k], t_sem.at[4, k], t_sem.at[5, 4 - k], (sp, 2 * there + c)
-            )
-            copy.start()
-            tails.append(copy)
-        else:
-            sums = value
-    for k in (1, 3, 2):
-        remote(row_s.at[k - 1], row_r.at[k - 1], t_sem.at[4, k], t_sem.at[5, k], (sp, partner)).wait_recv()
-        sums = sums + row_r[k - 1].astype(F32)
+    tails = exchange(cat, cat_r, 6)
+    sums = dot(cat[tp], w_o[c], ((1,), (0,)))
+    pass_on(4)
+    pass_on(5)
+    for k in (0, 1, 3, 2):
+        for core in (1 - c, c):
+            if k == 0 and core is c:
+                continue
+            member = 2 * lax.rem(y + k, 4) + core
+            if core is not c:
+                for part in (0, 1):
+                    acrosses[k, part].wait_recv()
+            away = lax.rem(member - tp + 8, 8)
+            remote(
+                cat_r.at[member], cat_r.at[member], g_sem.at[6, away], g_sem.at[7, away], (sp, partner)
+            ).wait_recv()
+            sums = sums + dot(cat_r[member], w_o[2 * k + core], ((1,), (0,)))
     out[...] = sums.astype(BF)
 
-    for copy in gathers + halos + tails:
+    for copy in gathers + halos + tails + rounds + list(acrosses.values()):
         copy.wait_send()
     for core in (0, 1):
 
@@ -430,7 +486,7 @@
             pltpu.VMEM((2048, 256), BF),
             pltpu.VMEM((32, 2048), BF),
             pltpu.VMEM((2048, 512), BF),
-            pltpu.VMEM((256, 2048), BF),
+            pltpu.VMEM((8, 256, 2048), BF),
             pltpu.VMEM((8, OWN, TB), BF),
             pltpu.VMEM((8, OWN, 512), BF),
             pltpu.VMEM((8, OWN, 128), BF),
@@ -445,17 +501,16 @@
             pltpu.VMEM((H, TB, 128), F32),
             pltpu.VMEM((TB, 64), BF),
             pltpu.VMEM((8, OWN, 256), BF),
-            pltpu.VMEM((4, OWN, 2048), BF),
-            pltpu.VMEM((4, OWN, 2048), BF),
-            pltpu.VMEM((4, OWN, 2048), F32),
-            pltpu.VMEM((3, OWN, 2048), BF),
-            pltpu.VMEM((3, OWN, 2048), BF),
+            pltpu.VMEM((8, OWN, 256), BF),
             dma((6,)),
-            dma((6, 8)),
+            dma((8, 8)),
             dma((NB, 6)),
             dma((NB,)),
             dma((NB,)),
-            dma((6, 4)),
+            dma((14,)),
+            dma((6,)),
+            dma((8,)),
+            dma((2, 2)),
         ],
         compiler_params=pltpu.CompilerParams(
             collective_id=0, has_side_effects=True, vmem_limit_bytes=60 * 2**20

time: 77.2 us -> 66.6 us (0.86)
  Pallas kernels: 73.5 us -> 62.9 us
    pallas_call x1, Pallas kernels: 73.5 us -> 62.9 us  [shards(): pl.pallas_call(layer, out_shape=(jax.ShapeDtypeStruct((OWN, 2048), BF), j...]
where the time goes in v3:
time: 66.6 us; the launch traced here: 66.4 us
  Pallas kernels  62.9 us (94%)
  local copies, waits for them, and re-layouts  2.9 us (4%)
    pallas_call x1, Pallas kernels, shards(): pl.pallas_call(layer, out_shape=(jax.ShapeDtypeStruct((OWN, 2048), BF), j...  62.9 us
    unnamed x2, local copies, waits for them, and re-layouts  2.9 us

profile of v3, /device:TPU:1, one launch (start us, length us, event | category | flops | bytes accessed | tf_op | source)
XLA Modules:
  0.0 66.4 jit_solution(2215808211799616261)
XLA Ops:
  0.6 62.9 %layer.1 = (bf16[48,2048]{1,0:T(8,128)(2,1)}, f32[3,384]{1,0:T(4,128)}) custom-call(bf16[48,2048]{1,0:T(8,128)(2,1)} %tok.1, bf16[2048,512]{1,0:T(8,128)(2,1)} %h_wq.1, bf16[2048,256]{1,0:T(8,128)(2,1)} %h_wkv.1, bf16[32,2048]{1,0:T(8,128)(2,1)} %bitcast.9, bf16[2048,512]{1,0:T(8,128)(2,1)} %h_wp.1, bf16[16,128]{1,0:T(8,128)(2,1)} %bitcast.10, ...), custom_call_target="tpu_custom_call" | custom-call | tf_op jit(solution)/shard_map/layer/pallas_call | solution.py:479
  63.5 1.6 %copy.21 = bf16[48,2048]{1,0:T(8,128)(2,1)} copy(bf16[48,2048]{1,0:T(8,128)(2,1)} %get-tuple-element.4) | data formatting | bytes 393216
  65.1 1.3 %copy.22 = f32[3,384]{1,0:T(4,128)} copy(f32[3,384]{1,0:T(4,128)} %get-tuple-element.5) | data formatting | bytes 9216

commit v4 on v3

--- a/solution.py
+++ b/solution.py
@@ -128,7 +128,7 @@
     w_mix, p_scale, h_woa, h_wop,
     out, lse_out,
     w_q, w_kv, w_r, w_p, w_o, kvg, qg, psend, pool, halo, lat, qs, wup, k_ref, v_ref, m_ref, acc,
-    pool_out, cat, cat_r,
+    s_ref, pool_out, cat, cat_r,
     w_sem, g_sem, lat_send, lat_recv, pair_recv, o_send, o_recv, o_pair, t_sem,
 ):
     sp, tp = lax.axis_index("sp"), lax.axis_index("tp")
@@ -271,7 +271,8 @@
     acc[...] = jnp.zeros(acc.shape, F32)
     k_ref[...] = jnp.zeros(k_ref.shape, BF)
     v_ref[...] = jnp.zeros(v_ref.shape, BF)
-    v_ref[:, 64:80, :] = jnp.ones((H, 16, v_ref.shape[2]), BF)
+    v_ref[:, :, 64:80, :] = jnp.ones((2, H, 16, v_ref.shape[3]), BF)
+    s_ref[...] = jnp.full(s_ref.shape, -3e38, F32)
 
     gathers += gathered(kvg, 0)
     turned = jnp.transpose(kvg[...].reshape(TB, TB).astype(F32))
@@ -402,53 +403,59 @@
                             lat.at[s, 1 - c], lat.at[s, 1 - c], lat_send.at[s, 5], pair_recv.at[s], (sp, partner)
                         ).wait_recv()
 
+        def between(h):
+            for k in range(STEPS):
+                if any(SERVICE[core][3 * k + h] for core in (0, 1)):
+
+                    @pl.when(i == k)
+                    def _():
+                        serve(3 * k + h)
+
+        v_now, v_last = v_ref.at[lax.rem(i, 2)], v_ref.at[1 - lax.rem(i, 2)]
         for j in range(PER):
-            prep(lat[i * PER + j].reshape(2 * LH, TB), wup, k_ref, v_ref, j * TB)
-        held = None
-        for h in range(H):
-            s = dot(qs[h], k_ref[h], ((1,), (0,)))
-            if held is not None:
-                soften(h - 1, held, m_ref, acc, v_ref)
-            held = s
-            if h < H - 1:
-                for k in range(STEPS):
-                    if any(SERVICE[core][3 * k + h + 1] for core in (0, 1)):
-
-                        @pl.when(i == k)
-                        def _():
-                            serve(3 * k + h + 1)
-
-        soften(H - 1, held, m_ref, acc, v_ref)
+            prep(lat[i * PER + j].reshape(2 * LH, TB), wup, k_ref, v_now, j * TB)
+        s_0 = dot(qs[0], k_ref[0], ((1,), (0,)))
+        soften(2, s_ref[...], m_ref, acc, v_last)
+        between(1)
+        s_1 = dot(qs[1], k_ref[1], ((1,), (0,)))
+        soften(0, s_0, m_ref, acc, v_now)
+        between(2)
+        s_ref[...] = dot(qs[2], k_ref[2], ((1,), (0,)))
+        soften(1, s_1, m_ref, acc, v_now)
         return carry
 
     lax.fori_loop(0, STEPS, step, 0)
 
+    def head_out(h):
+        o = acc[h]
+        return (o[:, :64] / o[:, 64:65]).astype(BF)
+
+    cat[0] = jnp.concatenate([head_out(0), head_out(1)], axis=1).reshape(8, OWN, 128)
+    tails = exchange(cat.at[0], cat_r.at[0], 6)
+    soften(2, s_ref[...], m_ref, acc, v_ref.at[(STEPS - 1) % 2])
+    cat[1] = jnp.concatenate([head_out(2), pool_out[...]], axis=1).reshape(8, OWN, 128)
+    tails += exchange(cat.at[1], cat_r.at[1], 8)
     lane = lax.broadcasted_iota(jnp.int32, (TB, 128), 1)
-    parts, logs = [], jnp.zeros((TB, 128), F32)
+    logs = jnp.zeros((TB, 128), F32)
     for h in range(H):
-        o = acc[h]
-        total = o[:, 64:65]
-        parts.append((o[:, :64] / total).astype(BF))
-        logs = jnp.where(lane == h, m_ref[h] * LN2 + jnp.log(total), logs)
+        logs = jnp.where(lane == h, m_ref[h] * LN2 + jnp.log(acc[h][:, 64:65]), logs)
     lse_out[...] = jnp.transpose(logs)[:H]
-    cat[...] = jnp.concatenate(parts + [pool_out[...]], axis=1).reshape(8, OWN, 256)
-    tails = exchange(cat, cat_r, 6)
-    sums = dot(cat[tp], w_o[c], ((1,), (0,)))
+    sums = dot(cat[0, tp], w_o[c, :128], ((1,), (0,))) + dot(cat[1, tp], w_o[c, 128:], ((1,), (0,)))
     pass_on(4)
     pass_on(5)
-    for k in (0, 1, 3, 2):
-        for core in (1 - c, c):
-            if k == 0 and core is c:
-                continue
-            member = 2 * lax.rem(y + k, 4) + core
-            if core is not c:
-                for part in (0, 1):
+    for part in (0, 1):
+        for k in (0, 1, 3, 2):
+            for core in (1 - c, c):
+                if k == 0 and core is c:
+                    continue
+                member = 2 * lax.rem(y + k, 4) + core
+                if core is not c:
                     acrosses[k, part].wait_recv()
-            away = lax.rem(member - tp + 8, 8)
-            remote(
-                cat_r.at[member], cat_r.at[member], g_sem.at[6, away], g_sem.at[7, away], (sp, partner)
-            ).wait_recv()
-            sums = sums + dot(cat_r[member], w_o[2 * k + core], ((1,), (0,)))
+                away = lax.rem(member - tp + 8, 8)
+                here, kind = cat_r.at[part, member], 6 + 2 * part
+                remote(here, here, g_sem.at[kind, away], g_sem.at[kind + 1, away], (sp, partner)).wait_recv()
+                rows = slice(128 * part, 128 * part + 128)
+                sums = sums + dot(cat_r[part, member], w_o[2 * k + core, rows], ((1,), (0,)))
     out[...] = sums.astype(BF)
 
     for copy in gathers + halos + tails + rounds + list(acrosses.values()):
@@ -460,6 +467,11 @@
             for s in range(NB):
                 for copy in outgoing(core, s):
                     copy.wait_send()
+
+
+def write_out(mixed, logs, mixed_out, logs_out):
+    mixed_out[...] = mixed[...]
+    logs_out[...] = logs[...]
 
 
 def rotation_tables():
@@ -476,7 +488,7 @@
            query_gain, key_gain, w_pool_mix, pool_scale, w_out_attn, w_out_pool):
     vmem, anywhere = pl.BlockSpec(memory_space=pltpu.VMEM), pl.BlockSpec(memory_space=pl.ANY)
     dma, n = pltpu.SemaphoreType.DMA, PER * TB
-    return pl.pallas_call(
+    mixed, logs = pl.pallas_call(
         layer,
         out_shape=(jax.ShapeDtypeStruct((OWN, 2048), BF), jax.ShapeDtypeStruct((H, TB), F32)),
         in_specs=[vmem] + [anywhere] * 4 + [vmem] * 10 + [anywhere] * 2,
@@ -496,14 +508,15 @@
             pltpu.VMEM((H, TB, 128), BF),
             pltpu.VMEM((H * 128, 256), BF),
             pltpu.VMEM((H, 128, n), BF),
-            pltpu.VMEM((H, 128, n), BF),
+            pltpu.VMEM((2, H, 128, n), BF),
             pltpu.VMEM((H, TB, 128), F32),
             pltpu.VMEM((H, TB, 128), F32),
+            pltpu.VMEM((TB, n), F32),
             pltpu.VMEM((TB, 64), BF),
-            pltpu.VMEM((8, OWN, 256), BF),
-            pltpu.VMEM((8, OWN, 256), BF),
+            pltpu.VMEM((2, 8, OWN, 128), BF),
+            pltpu.VMEM((2, 8, OWN, 128), BF),
             dma((6,)),
-            dma((8, 8)),
+            dma((10, 8)),
             dma((NB, 6)),
             dma((NB,)),
             dma((NB,)),
@@ -522,6 +535,13 @@
         query_up_weight.T, key_value_up_weight, query_gain[None], key_gain[None],
         jnp.asarray(rotation_tables()), w_pool_mix, pool_scale[None], w_out_attn, w_out_pool,
     )
+    return pl.pallas_call(
+        write_out,
+        out_shape=(jax.ShapeDtypeStruct((OWN, 2048), BF), jax.ShapeDtypeStruct((H, TB), F32)),
+        in_specs=[vmem] * 2,
+        out_specs=(vmem, vmem),
+        name="write_out",
+    )(mixed, logs)
 
 
 def solution(mesh):

time: 66.6 us -> 65.2 us (0.979)
  local copies, waits for them, and re-layouts: 2.9 us -> 0 us
  Pallas kernels: 62.9 us -> 64.4 us
    unnamed x2 -> x0, local copies, waits for them, and re-layouts: 2.9 us -> none
    pallas_call x0 -> x1, Pallas kernels: none -> 1.62 us  [shards(): pl.pallas_call(write_out, out_shape=(jax.ShapeDtypeStruct((OWN, 2048), BF...]
where the time goes in v4:
time: 65.2 us; the launch traced here: 65.1 us
  Pallas kernels  64.4 us (99%)
    pallas_call x1, Pallas kernels, shards(): pl.pallas_call(layer, out_shape=(jax.ShapeDtypeStruct((OWN, 2048), BF), j...  62.8 us
    pallas_call x1, Pallas kernels, shards(): pl.pallas_call(write_out, out_shape=(jax.ShapeDtypeStruct((OWN, 2048), BF...  1.62 us

profile of v4, /device:TPU:1, one launch (start us, length us, event | category | flops | bytes accessed | tf_op | source)
XLA Modules:
  0.0 65.1 jit_solution(7913871569625477196)
XLA Ops:
  0.6 62.8 %layer.1 = (bf16[48,2048]{1,0:T(8,128)(2,1)}, f32[3,384]{1,0:T(4,128)}) custom-call(bf16[48,2048]{1,0:T(8,128)(2,1)} %tok.1, bf16[2048,512]{1,0:T(8,128)(2,1)} %h_wq.1, bf16[2048,256]{1,0:T(8,128)(2,1)} %h_wkv.1, bf16[32,2048]{1,0:T(8,128)(2,1)} %bitcast.9, bf16[2048,512]{1,0:T(8,128)(2,1)} %h_wp.1, bf16[16,128]{1,0:T(8,128)(2,1)} %bitcast.10, ...), custom_call_target="tpu_custom_call" | custom-call | tf_op jit(solution)/shard_map/layer/pallas_call | solution.py:491
  63.5 1.6 %write_out.1 = (bf16[48,2048]{1,0:T(8,128)(2,1)}, f32[3,384]{1,0:T(4,128)}) custom-call(bf16[48,2048]{1,0:T(8,128)(2,1)} %get-tuple-element.4.mixed, f32[3,384]{1,0:T(4,128)} %get-tuple-element.5.logs), custom_call_target="tpu_custom_call" | custom-call | tf_op jit(solution)/shard_map/write_out/pallas_call | solution.py:538

commit v5 on v4

--- a/solution.py
+++ b/solution.py
@@ -22,14 +22,14 @@
 LENGTH = NB * TB
 
 ORDER = (
-    (0, 0), (0, 1), (-1, 0), (1, 0),
-    (2, 0), (0, 3), (-1, 3), (-2, 0),
-    (1, 1), (1, 3), (0, 2), (-1, 1),
-    (2, 3), (-1, 2), (-3, 0), (3, 0),
-    (1, 2), (-2, 1), (2, 1), (-2, 3),
-    (-2, 2), (3, 3), (3, 1), (4, 0),
-    (-3, 3), (-3, 1), (2, 2), (4, 3),
-    (-3, 2), (4, 2), (4, 1), (3, 2),
+    (0, 0), (1, 0), (-1, 0), (0, 3),
+    (0, 1), (2, 0), (1, 3), (-2, 0),
+    (-1, 3), (1, 1), (-3, 0), (3, 0),
+    (-1, 1), (2, 3), (-1, 2), (0, 2),
+    (-2, 3), (1, 2), (4, 0), (3, 3),
+    (-2, 1), (-3, 3), (2, 1), (2, 2),
+    (-2, 2), (4, 3), (-3, 1), (3, 2),
+    (3, 1), (-3, 2), (4, 1), (4, 2),
 )
 NEAR = ((1, 0), (-1, 0), (0, 1), (0, -1))
 
@@ -65,14 +65,14 @@
     for core in (0, 1)
 )
 SERVICE = (
-    ((2, 3, 5, 1), (), (), (7, 4, 10, 6, 9), (), (11, 8), (), (14, 15), (13, 16), (19, 12), (), (18,), (17,),
-     (26, 23), (21,), (20, 22), (24,), (25, 31), (27,), (28,), (), (30, 29), (), ()),
-    ((2, 3, 5, 1), (), (), (11, 7, 4, 6, 8, 9), (10, 13), (19, 17), (14, 15, 12), (18,), (16,), (20,), (25, 24),
-     (23, 22, 21), (), (26,), (), (28, 27), (30,), (31,), (), (29,), (), (), (), ()),
+    ((2, 1, 3, 4), (), (), (7, 5, 15, 8, 6), (12, 9), (), (10, 11, 14, 17), (16, 13), (22,), (20,), (23,),
+     (18, 19), (24,), (28, 21), (27,), (26,), (25, 29), (), (31,), (30,), (), (), (), ()),
+    ((2, 1, 3, 4), (), (), (12, 7, 5, 8, 9, 6), (15, 14), (16, 20), (10, 11, 13, 22), (17,), (24,), (26, 21),
+     (18, 28, 19), (), (23,), (29,), (25, 30), (27,), (), (), (31,), (), (), (), (), ()),
 )
 
 
-W_STEPS = {4: (0, 1), 7: (2, 3)}
+W_STEPS = {4: (0, 1)}
 
 
 def dot(a, b, dims):
@@ -369,62 +369,61 @@
         mapped = dot(pooled[:, :64], w_mix[0], ((1,), (0,)))
         pool_out[...] = (mapped * p_scale[...].astype(F32)).astype(BF)
 
+    v_own = v_ref.at[1, :, :, pl.ds(0, TB)]
+    prep(lat[0].reshape(2 * LH, TB), wup, k_ref, v_own, 0)
+    held = [dot(qs[h], k_ref[h, :, :TB], ((1,), (0,))) for h in range(H)]
+    for h in range(H):
+        soften(h, held[h], m_ref, acc, v_own)
+
+    def arrive(k):
+        if k == 1:
+            pooling()
+        for i_round in W_STEPS.get(k, ()):
+            pass_on(i_round)
+        serve(3 * k)
+        for s in range(PER * k + 1, min(PER * k + PER + 1, NB)):
+            remote(
+                lat.at[s, 1 - c], lat.at[s, 1 - c], lat_send.at[s, 5], pair_recv.at[s], (sp, partner)
+            ).wait_recv()
+
+    def heads(first, count, v_now, v_last, between):
+        n = count * TB
+        block = jnp.concatenate([lat[first + j].reshape(2 * LH, TB) for j in range(count)], axis=1)
+        prep(block, wup, k_ref, v_now, 0)
+        s_0 = dot(qs[0], k_ref[0, :, :n], ((1,), (0,)))
+        soften(2, s_ref[...], m_ref, acc, v_last)
+        between(1)
+        s_1 = dot(qs[1], k_ref[1, :, :n], ((1,), (0,)))
+        soften(0, s_0, m_ref, acc, v_now)
+        between(2)
+        s_2 = dot(qs[2], k_ref[2, :, :n], ((1,), (0,)))
+        soften(1, s_1, m_ref, acc, v_now)
+        return s_2
+
     def step(i, carry):
-        for k in range(STEPS):
+        for k in range(STEPS - 1):
 
             @pl.when(i == k)
             def _():
-                if k == 1:
-                    pooling()
-                for i_round in W_STEPS.get(k, ()):
-                    pass_on(i_round)
-                if k:
-                    serve(3 * k)
-                else:
-                    for core in (0, 1):
-
-                        @pl.when(c == core)
-                        def _():
-                            for s in SERVICE[core][0]:
-                                if s:
-                                    remote(
-                                        lat.at[s, core],
-                                        lat.at[s, core],
-                                        lat_send.at[s, 0],
-                                        lat_recv.at[s],
-                                        (sp, partner),
-                                    ).wait_recv()
-                                    for copy in outgoing(core, s):
-                                        copy.start()
-
-                for s in range(PER * k, PER * k + PER):
-                    if s:
-                        remote(
-                            lat.at[s, 1 - c], lat.at[s, 1 - c], lat_send.at[s, 5], pair_recv.at[s], (sp, partner)
-                        ).wait_recv()
+                arrive(k)
 
         def between(h):
-            for k in range(STEPS):
+            for k in range(STEPS - 1):
                 if any(SERVICE[core][3 * k + h] for core in (0, 1)):
 
                     @pl.when(i == k)
                     def _():
                         serve(3 * k + h)
 
-        v_now, v_last = v_ref.at[lax.rem(i, 2)], v_ref.at[1 - lax.rem(i, 2)]
-        for j in range(PER):
-            prep(lat[i * PER + j].reshape(2 * LH, TB), wup, k_ref, v_now, j * TB)
-        s_0 = dot(qs[0], k_ref[0], ((1,), (0,)))
-        soften(2, s_ref[...], m_ref, acc, v_last)
-        between(1)
-        s_1 = dot(qs[1], k_ref[1], ((1,), (0,)))
-        soften(0, s_0, m_ref, acc, v_now)
-        between(2)
-        s_ref[...] = dot(qs[2], k_ref[2], ((1,), (0,)))
-        soften(1, s_1, m_ref, acc, v_now)
+        now = lax.rem(i, 2)
+        s_ref[...] = heads(i * PER + 1, PER, v_ref.at[now], v_ref.at[1 - now], between)
         return carry
 
-    lax.fori_loop(0, STEPS, step, 0)
+    lax.fori_loop(0, STEPS - 1, step, 0)
+    arrive(STEPS - 1)
+    last = (STEPS - 1) * PER + 1
+    v_end = v_ref.at[(STEPS - 1) % 2, :, :, pl.ds(0, (NB - last) * TB)]
+    s_end = heads(last, NB - last, v_end, v_ref.at[STEPS % 2], lambda h: serve(3 * (STEPS - 1) + h))
 
     def head_out(h):
         o = acc[h]
@@ -432,7 +431,9 @@
 
     cat[0] = jnp.concatenate([head_out(0), head_out(1)], axis=1).reshape(8, OWN, 128)
     tails = exchange(cat.at[0], cat_r.at[0], 6)
-    soften(2, s_ref[...], m_ref, acc, v_ref.at[(STEPS - 1) % 2])
+    pass_on(2)
+    pass_on(3)
+    soften(2, s_end, m_ref, acc, v_end)
     cat[1] = jnp.concatenate([head_out(2), pool_out[...]], axis=1).reshape(8, OWN, 128)
     tails += exchange(cat.at[1], cat_r.at[1], 8)
     lane = lax.broadcasted_iota(jnp.int32, (TB, 128), 1)

time: 65.2 us -> 64.1 us (0.983)
  Pallas kernels: 64.4 us -> 63.4 us
    pallas_call x1, Pallas kernels: 62.8 us -> 61.8 us  [shards(): pl.pallas_call(layer, out_shape=(jax.ShapeDtypeStruct((OWN, 2048), BF), j...]
where the time goes in v5:
time: 64.1 us; the launch traced here: 64 us
  Pallas kernels  63.4 us (99%)
  between operations  0.65 us (1%)
    pallas_call x1, Pallas kernels, shards(): pl.pallas_call(layer, out_shape=(jax.ShapeDtypeStruct((OWN, 2048), BF), j...  61.8 us
    pallas_call x1, Pallas kernels, shards(): pl.pallas_call(write_out, out_shape=(jax.ShapeDtypeStruct((OWN, 2048), BF...  1.62 us

profile of v5, /device:TPU:1, one launch (start us, length us, event | category | flops | bytes accessed | tf_op | source)
XLA Modules:
  0.0 64.0 jit_solution(12516356501976203330)
XLA Ops:
  0.6 61.8 %layer.1 = (bf16[48,2048]{1,0:T(8,128)(2,1)}, f32[3,384]{1,0:T(4,128)}) custom-call(bf16[48,2048]{1,0:T(8,128)(2,1)} %tok.1, bf16[2048,512]{1,0:T(8,128)(2,1)} %h_wq.1, bf16[2048,256]{1,0:T(8,128)(2,1)} %h_wkv.1, bf16[32,2048]{1,0:T(8,128)(2,1)} %bitcast.9, bf16[2048,512]{1,0:T(8,128)(2,1)} %h_wp.1, bf16[16,128]{1,0:T(8,128)(2,1)} %bitcast.10, ...), custom_call_target="tpu_custom_call" | custom-call | tf_op jit(solution)/shard_map/layer/pallas_call | solution.py:492
  62.4 1.6 %write_out.1 = (bf16[48,2048]{1,0:T(8,128)(2,1)}, f32[3,384]{1,0:T(4,128)}) custom-call(bf16[48,2048]{1,0:T(8,128)(2,1)} %get-tuple-element.4.mixed, f32[3,384]{1,0:T(4,128)} %get-tuple-element.5.logs), custom_call_target="tpu_custom_call" | custom-call | tf_op jit(solution)/shard_map/write_out/pallas_call | solution.py:539
